TPU v7x, 32 devices: a whole 2x2x4 slice. The times are simulated.
32 devices in a mesh: sp: 16 (over z, y, x), tp: 2 (over core).
Axes of the slice: x: 2, y: 2, z: 4, core: 2. Of those that a mesh axis runs over, the one named last changes fastest.
Arguments:
- queries_narrow: bfloat16 [4096, 1024], P('sp', 'tp'), may hold values from -40 to 40
- keys_narrow: bfloat16 [4096, 256], P('sp', 'tp'), may hold values from -40 to 40
- values_narrow: bfloat16 [4096, 256], P('sp', 'tp'), may hold values from -6 to 6
- queries_wide: bfloat16 [4096, 1024], P('sp', 'tp'), may hold values from -40 to 40
- keys_wide: bfloat16 [4096, 512], P('sp', 'tp'), may hold values from -40 to 40
- values_wide: bfloat16 [4096, 512], P('sp', 'tp'), may hold values from -6 to 6
- lambda_narrow: float32 [8], P('tp'), may hold values from 0.3 to 0.8
- lambda_wide: float32 [4], P('tp'), may hold values from 0.3 to 0.8
- gain_narrow: float32 [128], replicated, may hold values from 0.1 to 1.9
- gain_wide: float32 [256], replicated, may hold values from 0.1 to 1.9
- out_narrow: bfloat16 [1024, 2048], replicated, may hold values from -0.125 to 0.125
- out_wide: bfloat16 [1024, 2048], replicated, may hold values from -0.125 to 0.125
- stream: bfloat16 [4096, 2048], P(('sp', 'tp')), may hold values from -6 to 6
- gain_mix: float32 [2048], replicated, may hold values from 0.1 to 1.9
- gain_ffn: float32 [2048], replicated, may hold values from 0.1 to 1.9
- gain_post: float32 [2048], replicated, may hold values from 0.1 to 1.9
- shared_gate: bfloat16 [2048, 512], replicated, may hold values from -0.125 to 0.125
- shared_up: bfloat16 [2048, 512], replicated, may hold values from -0.125 to 0.125
- shared_down: bfloat16 [512, 2048], replicated, may hold values from -0.25 to 0.25
- expert_gate: bfloat16 [32, 2048, 512], P('sp', None, 'tp'), may hold values from -0.125 to 0.125
- expert_up: bfloat16 [32, 2048, 512], P('sp', None, 'tp'), may hold values from -0.125 to 0.125
- expert_down: bfloat16 [32, 512, 2048], P('sp', 'tp'), may hold values from -0.25 to 0.25
- expert_ids: int32 [4096, 4], P(('sp', 'tp')), may hold values from 0 to 31, all different within a row; in each aligned block of 128 rows (0 to 127, 128 to 255, ...) at most 24 rows name the same one
- route_weights: float32 [4096, 4], P(('sp', 'tp')), may hold values from 0.2 to 1
Outputs:
- layer_out: bfloat16 [4096, 2048], P(('sp', 'tp'))
Inputs may be any that keep to these rules, and one draw needn't show every extreme that they name: `expert_ids`: the experts of one token differ. Within the rows that one device holds (aligned blocks of rows in the placement's order), no expert is named more than 24 times, and in every draw some expert is named exactly 24 times there.
All inputs are finite; a program needn't handle non-finite values.
Results may differ from a plain program's by a relative error of at most 0.015.
Values may be sent and summed in bfloat16 or wider, within the bound.
A program may use at most 192 MiB of HBM per device.

v0:
```python
import math

import jax
import jax.numpy as jnp
from jax import lax
from jax.sharding import PartitionSpec as P

D = 2048
DN = 64
VN = 128
DW = 128
VW = 256
TOPK = 4


EPS = 1e-06


def rms_scale(values, gain_row):
    return values * lax.rsqrt(jnp.mean(values * values, axis=-1, keepdims=True) + EPS) * gain_row


def empty_state(groups, per_group, query_count, value_dim):
    return (
        jnp.full((groups, per_group, 2, query_count), -1e30, jnp.float32),
        jnp.zeros((groups, per_group, 2, query_count), jnp.float32),
        jnp.zeros((groups, per_group, 2, query_count, value_dim), jnp.float32),
    )


def attend_block(carried, query_heads, key_rows, value_rows, query_pos, key_pos, key_dim):
    row_max, row_sum, accumulated = carried
    scores = jnp.einsum(
        "qcgmd,kcmd->cgmqk", query_heads, key_rows, preferred_element_type=jnp.float32
    ) * key_dim ** (-0.5)
    causal = key_pos[None, :] <= query_pos[:, None]
    scores = jnp.where(causal, scores, -1e30)
    newmax = jnp.maximum(row_max, jnp.max(scores, axis=-1))
    weights = jnp.where(causal, jnp.exp(scores - newmax[..., None]), 0.0)
    factor = jnp.exp(row_max - newmax)
    row_sum = row_sum * factor + jnp.sum(weights, axis=-1)
    accumulated = accumulated * factor[..., None] + jnp.einsum(
        "cgmqk,kcv->cgmqv",
        weights.astype(jnp.bfloat16),
        value_rows,
        preferred_element_type=jnp.float32,
    )
    return (newmax, row_sum, accumulated)


def finish_group(carried, lam_heads, gain_row, value_dim):
    row_max, row_sum, accumulated = carried
    mapped = accumulated / row_sum[..., None]
    groups = mapped.shape[0]
    per_group = mapped.shape[1]
    lam_grid = lam_heads.reshape(groups, per_group)[:, :, None, None]
    difference = mapped[:, :, 0] - lam_grid * mapped[:, :, 1]
    normed = rms_scale(difference, gain_row)
    query_count = normed.shape[2]
    return (
        normed.transpose(2, 0, 1, 3)
        .reshape(query_count, groups * per_group * value_dim)
        .astype(jnp.bfloat16)
    )


def run_experts(incoming, expert_gate, expert_up, expert_down, capacity):
    sources = incoming.shape[0]
    local_experts = expert_gate.shape[0]
    grouped = incoming.reshape(sources, local_experts, capacity, D)
    gate_part = jnp.einsum(
        "rjcd,jdf->rjcf", grouped, expert_gate, preferred_element_type=jnp.float32
    )
    up_part = jnp.einsum("rjcd,jdf->rjcf", grouped, expert_up, preferred_element_type=jnp.float32)
    hidden = (jax.nn.silu(gate_part) * up_part).astype(jnp.bfloat16)
    result = jnp.einsum("rjcf,jfd->rjcd", hidden, expert_down, preferred_element_type=jnp.float32)
    return result.reshape(sources, local_experts * capacity, D)


def shards(
    queries_narrow,
    keys_narrow,
    values_narrow,
    queries_wide,
    keys_wide,
    values_wide,
    lambda_narrow,
    lambda_wide,
    gain_narrow,
    gain_wide,
    out_narrow,
    out_wide,
    stream,
    gain_mix,
    gain_ffn,
    gain_post,
    shared_gate,
    shared_up,
    shared_down,
    expert_gate,
    expert_up,
    expert_down,
    expert_ids,
    route_weights,
):
    query_count = queries_narrow.shape[0]
    sp_index = lax.axis_index("sp")
    sp_count = lax.axis_size("sp")
    offset = sp_index * query_count
    narrow_groups = keys_narrow.shape[1] // (2 * DN)
    wide_groups = keys_wide.shape[1] // (2 * DW)
    query_sets = (queries_narrow, queries_wide, offset + jnp.arange(query_count, dtype=jnp.int32))
    prepared = []
    narrow_part, wide_part, positions = query_sets
    rows = narrow_part.shape[0]
    prepared.append(
        (
            narrow_part.reshape(rows, narrow_groups, -1, 2, DN),
            wide_part.reshape(rows, wide_groups, -1, 2, DW),
            positions,
            positions[rows - 1],
        )
    )
    initial = tuple(
        (
            (
                empty_state(narrow_groups, item[0].shape[2], item[0].shape[0], VN),
                empty_state(wide_groups, item[1].shape[2], item[1].shape[0], VW),
            )
            for item in prepared
        )
    )
    pieces = (
        lax.all_gather(keys_narrow, "sp", axis=0, tiled=True),
        lax.all_gather(values_narrow, "sp", axis=0, tiled=True),
        lax.all_gather(keys_wide, "sp", axis=0, tiled=True),
        lax.all_gather(values_wide, "sp", axis=0, tiled=True),
    )
    key_count = pieces[0].shape[0]
    block_rows = math.gcd(key_count, 1024)
    narrow_keys = pieces[0].reshape(key_count, narrow_groups, 2, DN)
    narrow_values = pieces[1].reshape(key_count, narrow_groups, VN)
    wide_keys = pieces[2].reshape(key_count, wide_groups, 2, DW)
    wide_values = pieces[3].reshape(key_count, wide_groups, VW)

    def step_block(block_index, running):
        block_begin = block_index * block_rows
        key_pos = block_begin + jnp.arange(block_rows, dtype=jnp.int32)

        def take_rows(data):
            return lax.dynamic_slice_in_dim(data, block_begin, block_rows, 0)

        narrow_heads, wide_heads, positions, last_query = prepared[0]

        def update(
            carried_in, narrow_heads=narrow_heads, wide_heads=wide_heads, positions=positions
        ):
            return (
                attend_block(
                    carried_in[0],
                    narrow_heads,
                    take_rows(narrow_keys),
                    take_rows(narrow_values),
                    positions,
                    key_pos,
                    DN,
                ),
                attend_block(
                    carried_in[1],
                    wide_heads,
                    take_rows(wide_keys),
                    take_rows(wide_values),
                    positions,
                    key_pos,
                    DW,
                ),
            )

        def unchanged(carried_in):
            return carried_in

        updated = [lax.cond(block_begin <= last_query, update, unchanged, running[0])]
        return tuple(updated)

    states = lax.fori_loop(0, key_count // block_rows, step_block, initial)
    finished = [
        (
            finish_group(state[0], lambda_narrow, gain_narrow, VN),
            finish_group(state[1], lambda_wide, gain_wide, VW),
        )
        for state in states
    ]
    narrow_out, wide_out = finished[0]
    narrow_rows, wide_rows = (
        lax.all_to_all(narrow_out, "tp", split_axis=0, concat_axis=1, tiled=True),
        lax.all_to_all(wide_out, "tp", split_axis=0, concat_axis=1, tiled=True),
    )
    projected = jnp.dot(narrow_rows, out_narrow, preferred_element_type=jnp.float32) + jnp.dot(
        wide_rows, out_wide, preferred_element_type=jnp.float32
    )
    mixed_rows = (stream.astype(jnp.float32) + rms_scale(projected, gain_mix)).astype(jnp.bfloat16)
    normed = rms_scale(mixed_rows.astype(jnp.float32), gain_ffn).astype(jnp.bfloat16)
    row_count = normed.shape[0]
    tp_count = lax.axis_size("tp")
    local_experts = expert_gate.shape[0]
    experts_all = local_experts * sp_count
    capacity = max(2, 3 * row_count * TOPK // (2 * experts_all))
    flat_ids = expert_ids.reshape(-1)
    onehot = (flat_ids[:, None] == jnp.arange(experts_all, dtype=jnp.int32)[None, :]).astype(
        jnp.int32
    )
    earlier = jnp.cumsum(onehot, axis=0) - onehot
    slot_rank = jnp.sum(earlier * onehot, axis=1)
    slot_index = flat_ids * capacity + slot_rank
    buffer_rows = experts_all * capacity
    selector = slot_index[None, :] == jnp.arange(buffer_rows, dtype=jnp.int32)[:, None]
    selector = jnp.any(selector.reshape(buffer_rows, row_count, TOPK), axis=2).astype(jnp.bfloat16)
    outgoing = jnp.dot(selector, normed, preferred_element_type=jnp.float32).astype(jnp.bfloat16)
    outgoing = outgoing.reshape(sp_count, local_experts * capacity, D)
    incoming = lax.all_to_all(outgoing, "sp", split_axis=0, concat_axis=0, tiled=True)
    all_rows = lax.all_gather(incoming[None], "tp", axis=0, tiled=True)
    partials = run_experts(
        all_rows.reshape(tp_count * sp_count, local_experts * capacity, D),
        expert_gate,
        expert_up,
        expert_down,
        capacity,
    )
    partials = partials.reshape(tp_count, sp_count, local_experts * capacity, D)
    own_sums = lax.psum_scatter(
        partials.astype(jnp.bfloat16), "tp", scatter_dimension=0, tiled=True
    ).astype(jnp.float32)
    returned = lax.all_to_all(
        own_sums[0].astype(jnp.bfloat16), "sp", split_axis=0, concat_axis=0, tiled=True
    )
    returned = returned.reshape(buffer_rows, D)
    picked = jnp.take(returned, slot_index, axis=0).reshape(row_count, TOPK, D)
    routed = jnp.einsum(
        "rk,rkd->rd", route_weights, picked.astype(jnp.float32), precision=lax.Precision.HIGHEST
    )
    shared_hidden = (
        jax.nn.silu(jnp.dot(normed, shared_gate, preferred_element_type=jnp.float32))
        * jnp.dot(normed, shared_up, preferred_element_type=jnp.float32)
    ).astype(jnp.bfloat16)
    shared_out = jnp.dot(shared_hidden, shared_down, preferred_element_type=jnp.float32)
    combined = shared_out + routed
    return (mixed_rows.astype(jnp.float32) + rms_scale(combined, gain_post)).astype(jnp.bfloat16)


def solution(mesh):
    return jax.shard_map(
        shards,
        mesh=mesh,
        in_specs=(
            P("sp", "tp"),
            P("sp", "tp"),
            P("sp", "tp"),
            P("sp", "tp"),
            P("sp", "tp"),
            P("sp", "tp"),
            P("tp"),
            P("tp"),
            P(),
            P(),
            P(),
            P(),
            P(("sp", "tp"), None),
            P(),
            P(),
            P(),
            P(),
            P(),
            P(),
            P("sp", None, "tp"),
            P("sp", None, "tp"),
            P("sp", "tp", None),
            P(("sp", "tp"), None),
            P(("sp", "tp"), None),
        ),
        out_specs=P(("sp", "tp"), None),
        check_vma=False,
    )
```

profile of v0, /device:TPU:14, one launch (start us, length us, event | category | flops | bytes accessed | tf_op | source)
XLA Modules:
  0.0 573.1 jit_solution(14079362947930343164)
XLA Ops:
  16.4 48.2 %all-gather.7.cloned.1.call-done = bf16[4096,128]{1,0:T(8,128)(2,1)} async-done(((bf16[256,128]{1,0:T(8,128)(2,1)}), bf16[4096,128]{1,0:T(8,128)(2,1)}) %all-gather.7.cloned.1.call-update) | async-done | bytes 1048592 | tf_op jit(solution)/shard_map/all_gather | solution.py:134
  64.6 2.3 copy.118
  66.9 64.0 %all-gather.11.cloned.1.call-done = bf16[4096,256]{0,1:T(8,128)(2,1)} async-done(((bf16[256,256]{0,1:T(8,128)(2,1)}), bf16[4096,256]{0,1:T(8,128)(2,1)}) %all-gather.11.cloned.1.call-update) | async-done | bytes 2097168 | tf_op jit(solution)/shard_map/all_gather | solution.py:136
  130.9 4.1 copy.123
  135.0 52.2 %all-gather.9.cloned.1.call-done = bf16[4096,128]{1,0:T(8,128)(2,1)} async-done(((bf16[256,128]{1,0:T(8,128)(2,1)}), bf16[4096,128]{1,0:T(8,128)(2,1)}) %all-gather.9.cloned.1.call-update) | async-done | bytes 1048592 | tf_op jit(solution)/shard_map/all_gather | solution.py:135
  187.2 62.6 %all-gather.13.cloned.1.call-done = bf16[4096,256]{1,0:T(8,128)(2,1)} async-done(((bf16[256,256]{1,0:T(8,128)(2,1)}), bf16[4096,256]{1,0:T(8,128)(2,1)}) %all-gather.13.cloned.1.call-update) | async-done | bytes 2097168 | tf_op jit(solution)/shard_map/all_gather | solution.py:137
  252.0 31.6 %while.24 = (s32[]{:T(128)}, f32[1,4,2,256]{3,1,2,0:T(4,128)S(1)}, f32[1,4,2,256]{3,1,2,0:T(4,128)S(1)}, f32[1,4,2,256,128]{4,3,2,1,0:T(8,128)}, f32[1,2,2,256]{...) while((s32[]{:T(128)}, f32[1,4,2,256]{3,1,2,0:T(4,128)S(1)}, ...), condition=%wide.region_7.8_spmd.clone, body=%wide.region_0.7_spmd.clone.sunk | while | flops 1640245504 | bytes 62358096 | solution.py:185
  252.7 14.5 %conditional.3 = ((f32[1,4,2,256]{3,1,2,0:T(4,128)S(1)}, f32[1,4,2,256]{3,1,2,0:T(4,128)S(1)}, f32[1,4,2,256,128]{4,3,2,1,0:T(8,128)}, f32[1,2,2,256]{3,1,2,0:T(...) conditional(s32[]{:T(128)} %convert_element_type.156, (f32[1,4,2,256]{3,1,2,0:T(4,128)S(1)}, ...), branch_computations={%region_1.0_spmd, %region_2.6_spmd} | conditional | flops 1640245504 | bytes 62352608 | solution.py:182
  252.9 2.4 fusion.2
  255.3 2.3 fusion.5
  257.7 2.8 fusion.20
  260.6 2.2 fusion.8
  267.8 14.5 %conditional.3 = ((f32[1,4,2,256]{3,1,2,0:T(4,128)S(1)}, f32[1,4,2,256]{3,1,2,0:T(4,128)S(1)}, f32[1,4,2,256,128]{4,3,2,1,0:T(8,128)}, f32[1,2,2,256]{3,1,2,0:T(...) conditional(s32[]{:T(128)} %convert_element_type.156, (f32[1,4,2,256]{3,1,2,0:T(4,128)S(1)}, ...), branch_computations={%region_1.0_spmd, %region_2.6_spmd} | conditional | flops 1640245504 | bytes 62352608 | solution.py:182
  268.1 2.4 fusion.2
  270.5 2.3 fusion.5
  272.9 2.8 fusion.20
  286.9 5.0 all_to_all.42
  293.8 3.9 all_to_all.43
  298.0 3.1 fusion.102
  303.9 104.0 %all_to_all.44 = bf16[16,48,2048]{2,1,0:T(8,128)(2,1)} all-to-all(bf16[16,48,2048]{2,1,0:T(8,128)(2,1)S(1)} %bitcast.238), channel_id=1, replica_groups=mesh['sp'=16,'tp'=2] {'sp'}, dimensions={0} | all-to-all | bytes 6291456 | tf_op jit(solution)/shard_map/all_to_all | solution.py:220
  408.0 17.1 %all-gather.15.cloned.1.call-done = bf16[32,48,2048]{2,1,0:T(8,128)(2,1)} async-done(((bf16[16,48,2048]{2,1,0:T(8,128)(2,1)}), bf16[32,48,2048]{2,1,0:T(8,128)(2,1)}) %all-gather.15.cloned.1.call-update) | async-done | bytes 6291472 | tf_op jit(solution)/shard_map/all_gather | solution.py:221
  425.1 6.4 %fusion.46 = f32[2,32,24,256]{3,2,1,0:T(8,128)} fusion(bf16[32,2,24,2048]{3,2,1,0:T(8,128)(2,1)} %bitcast.255, bf16[2,2048,256]{2,1,0:T(8,128)(2,1)} %param.47), kind=kOutput, calls=%fused_computation.52 | convolution fusion | flops 1610612736 | bytes 9961472 | tf_op jit(solution)/shard_map/rjcd,jdf->rjcf/dot_general | solution.py:71
  431.5 10.1 %convert_bitcast_fusion = bf16[32,2,24,2048]{3,2,0,1:T(8,128)(2,1)} fusion(bf16[2,256,2048]{2,1,0:T(8,128)(2,1)S(1)} %copy-done, f32[2,32,24,256]{3,2,1,0:T(8,128)} %fusion.46, bf16[2,2048,256]{2,1,0:T(8,128)(2,1)} %param.48, bf16[32,2,24,2048]{3,2,1,0:T(8,128)(2,1)} %bitcast.256), kind=kOutput, calls=%fused_computation.49 | convolution fusion | flops 3226730496 | bytes 18350080 | tf_op jit(solution)/shard_map/rjcf,jfd->rjcd/dot_general | solution.py:76
  441.6 6.6 %copy.140 = bf16[32,2,24,2048]{3,2,1,0:T(8,128)(2,1)} copy(bf16[32,2,24,2048]{3,2,0,1:T(8,128)(2,1)} %convert_bitcast_fusion) | data formatting | bytes 12582912 | tf_op jit(solution)/shard_map/convert_element_type | solution.py:231
  448.2 16.2 %reduce-scatter.2.cloned.1.call-done = bf16[1,16,48,2048]{3,2,1,0:T(8,128)(2,1)} async-done(((bf16[2,16,48,2048]{3,2,1,0:T(8,128)(2,1)}), bf16[1,16,48,2048]{3,2,1,0:T(8,128)(2,1)}) %reduce-scatter.2.cloned.1.call-update) | async-done | bytes 3145744 | tf_op jit(solution)/shard_map/reduce_scatter | solution.py:230
  464.4 7.1 %all-to-all-start.3 = ((bf16[16,48,2048]{2,1,0:T(8,128)(2,1)}), bf16[16,48,2048]{2,1,0:T(8,128)(2,1)}, u32[]{:S(2)}, u32[]{:S(2)}) async-start(bf16[16,48,2048]{2,1,0:T(8,128)(2,1)} %bitcast.241), calls=%async_computation.4 | async-start | bytes 6291456 | tf_op jit(solution)/shard_map/all_to_all | solution.py:233
  474.1 67.6 %all-to-all-done.3 = bf16[16,48,2048]{2,1,0:T(8,128)(2,1)} async-done(((bf16[16,48,2048]{2,1,0:T(8,128)(2,1)}), bf16[16,48,2048]{2,1,0:T(8,128)(2,1)}, u32[]{:S(2)}, u32[]{:S(2)}) %all-to-all-start.3) | async-done | bytes 3145760 | tf_op jit(solution)/shard_map/all_to_all | solution.py:233
  541.7 7.5 %gather_fusion = bf16[512,2048]{1,0:T(8,128)(2,1)} fusion(bf16[768,2048]{1,0:T(8,128)(2,1)} %bitcast.63, s32[1024]{0:T(1024)S(1)} %pad_clamp_fusion), kind=kCustom, calls=%fused_computation | custom fusion | bytes 4196352 | tf_op jit(solution)/shard_map/jit(_take)/gather | solution.py:237
  549.2 4.1 gather.7
  553.3 6.1 %fusion.51 = f32[128,1,2048]{2,1,0:T(1,128)} fusion(f32[128,4,1]{1,2,0:T(1,128)S(1)} %copy.151, bf16[128,4,2048]{2,1,0:T(4,128)(2,1)} %gather.7, pred[128,4]{1,0:T(8,128)(4,1)S(1)} %copy.137), kind=kOutput, calls=%fused_computation.60 | convolution fusion | flops 13631488 | bytes 3148288 | tf_op jit(solution)/shard_map/rk,rkd->rd/dot_general | solution.py:238
  559.4 4.6 multiply_reduce_fusion
  564.0 2.3 fusion.71
  (149 shorter events, 33.9 us)
Async XLA Ops:
  6.5 425.0 %copy-start = (bf16[2,256,2048]{2,1,0:T(8,128)(2,1)S(1)}, bf16[2,256,2048]{2,1,0:T(8,128)(2,1)}, u32[]{:S(2)}) copy-start(bf16[2,256,2048]{2,1,0:T(8,128)(2,1)} %param.49) | copy-start | bytes 6291460
  6.5 9.6 %copy-start.10 = (s32[128,4]{0,1:T(4,128)S(1)}, s32[128,4]{0,1:T(4,128)}, u32[]{:S(2)}) copy-start(s32[128,4]{0,1:T(4,128)} %param.50) | copy-start | bytes 6148
  6.5 58.1 %all-gather.7.cloned.1.call-start = ((), (), s32[]{:S(2)}) async-start(), calls=%async_computation.5 | async-start | bytes 1114112 | tf_op jit(solution)/shard_map/all_gather | solution.py:134
  7.3 123.7 %all-gather.11.cloned.1.call-start = ((), (), s32[]{:S(2)}) async-start(), calls=%async_computation.7 | async-start | bytes 2228224 | tf_op jit(solution)/shard_map/all_gather | solution.py:136
  9.0 178.2 %all-gather.9.cloned.1.call-start = ((), (), s32[]{:S(2)}) async-start(), calls=%async_computation.6 | async-start | bytes 1114112 | tf_op jit(solution)/shard_map/all_gather | solution.py:135
  9.7 240.1 %all-gather.13.cloned.1.call-start = ((), (), s32[]{:S(2)}) async-start(), calls=%async_computation.8 | async-start | bytes 2228224 | tf_op jit(solution)/shard_map/all_gather | solution.py:137
  10.3 414.8 %all-gather.15.cloned.1.call-start = ((), (), s32[]{:S(2)}) async-start(), calls=%async_computation.10 | async-start | bytes 9437184 | tf_op jit(solution)/shard_map/all_gather | solution.py:221
  252.0 33.3 %copy-start.13 = (f32[4]{0:T(128)S(1)}, f32[4]{0:T(128)}, u32[]{:S(2)}) copy-start(f32[4]{0:T(128)} %param.34) | copy-start | bytes 52
  255.3 2.4 copy-start.1
  260.6 3.4 copy-start.2
  262.9 1.2 copy-start.3
  266.1 1.0 copy-start.4
  270.5 2.4 copy-start.1
  275.7 3.4 copy-start.2
  278.0 1.2 copy-start.3
  281.2 1.0 copy-start.4
  283.6 2.0 copy-start.17
  283.7 9.1 %copy-start.5 = (f32[1,2,2,256,256]{4,3,2,1,0:T(8,128)S(1)}, f32[1,2,2,256,256]{4,3,2,1,0:T(8,128)}, u32[]{:S(2)}) copy-start(f32[1,2,2,256,256]{4,3,2,1,0:T(8,128)} %get-tuple-element.332) | copy-start | bytes 3145732
  285.4 7.6 %copy-start.14 = (f32[2]{0:T(128)S(1)}, f32[2]{0:T(128)}, u32[]{:S(2)}) copy-start(f32[2]{0:T(128)} %param.35) | copy-start | bytes 28
  285.7 7.5 %copy-start.16 = (f32[256]{0:T(256)S(1)}, f32[256]{0:T(256)}, u32[]{:S(2)}) copy-start(f32[256]{0:T(256)} %param.37) | copy-start | bytes 3076
  292.8 5.2 copy-start.7
  298.0 3.5 copy-start.6
  301.4 1.0 copy-start.8
  301.4 1.0 copy-start.11
  301.4 1.4 copy-start.9
  408.0 56.5 %reduce-scatter.2.cloned.1.call-start = ((), (), s32[]{:S(2)}) async-start(), calls=%async_computation.9 | async-start | bytes 9437184 | tf_op jit(solution)/shard_map/reduce_scatter | solution.py:230
  464.4 7.1 %copy-start.15 = (f32[128,4]{0,1:T(4,128)S(1)}, f32[128,4]{0,1:T(4,128)}, u32[]{:S(2)}) copy-start(f32[128,4]{0,1:T(4,128)} %param.51) | copy-start | bytes 6148
  464.4 77.3 %all-to-all-start.3 = ((bf16[16,48,2048]{2,1,0:T(8,128)(2,1)}), bf16[16,48,2048]{2,1,0:T(8,128)(2,1)}, u32[]{:S(2)}, u32[]{:S(2)}) async-start(bf16[16,48,2048]{2,1,0:T(8,128)(2,1)} %bitcast.241), calls=%async_computation.4 | async-start | bytes 6291456 | tf_op jit(solution)/shard_map/all_to_all | solution.py:233
  559.4 4.6 copy-start.12
Sparse Core Ops, SparseCore 0:
  10.1 54.4 all-gather.6
  67.3 63.5 all-gather.10
  133.7 53.4 all-gather.8
  189.8 59.9 all-gather.12
  408.1 16.9 all-gather.14
  448.3 16.0 reduce-scatter.1
where the time goes:
time: 575 us; the launch traced here: 573 us
  waiting for transfers between devices  330 us (57%)
  blocking collectives  113 us (20%)
  matrix products  53.2 us (9%)
  local copies, waits for them, and re-layouts  38.5 us (7%)
  other arithmetic  14.5 us (3%)
  between operations  13.8 us (2%)
  starting transfers between devices  7.29 us (1%)
    all_to_all x1, blocking collectives, shards(): lax.all_to_all(outgoing, 'sp', split_axis=0, concat_axis=0, tiled=True)  104 us
    all_to_all x1, waiting for transfers between devices, shards(): lax.all_to_all(own_sums[0].astype(jnp.bfloat16), 'sp', split_axis=0, conc...  67.6 us
    all_gather x1, waiting for transfers between devices, shards(): lax.all_gather(keys_wide, 'sp', axis=0, tiled=True)  64 us
    all_gather x1, waiting for transfers between devices, shards(): lax.all_gather(values_wide, 'sp', axis=0, tiled=True)  62.6 us
    all_gather x1, waiting for transfers between devices, shards(): lax.all_gather(values_narrow, 'sp', axis=0, tiled=True)  52.2 us
    all_gather x1, waiting for transfers between devices, shards(): lax.all_gather(keys_narrow, 'sp', axis=0, tiled=True)  48.2 us
    all_gather x1, waiting for transfers between devices, shards(): all_rows = lax.all_gather(incoming[None], 'tp', axis=0, tiled=True)  17.1 us
    reduce_scatter x1, waiting for transfers between devices, shards(): lax.psum_scatter(partials.astype(jnp.bfloat16), 'tp', scatter_dimension=0...  16.2 us
  transfers between devices with their start and end apart: 7, of which 7 were waited for; matrix products, arithmetic and copies ran while one was open for 3% of the time, Pallas kernels for 0%

commit v1 on v0

v1 whole, which is shorter than its diff:
```python
import functools
import math

import jax
import jax.numpy as jnp
from jax import lax
from jax.experimental import pallas as pl
from jax.experimental.pallas import tpu as pltpu
from jax.sharding import PartitionSpec as P

D = 2048
DN = 64
VN = 128
DW = 128
VW = 256
TOPK = 4


EPS = 1e-06


def rms_scale(values, gain_row):
    return values * lax.rsqrt(jnp.mean(values * values, axis=-1, keepdims=True) + EPS) * gain_row


MESH = pl.DeviceIdType.MESH
LOG2E = math.log2(math.e)
MASKED = -1e30


def plane_shape(sp_count):
    bits = sp_count.bit_length() - 1
    if 1 << bits != sp_count:
        return sp_count, 1, 1
    columns = 1 << (bits // 3 if bits % 3 == 0 else (bits - bits // 2) // 2)
    rows = columns
    return sp_count // (rows * columns), rows, columns


def attend_kernel(
    dims,
    qn_ref,
    kn_ref,
    vn_ref,
    qw_ref,
    kw_ref,
    vw_ref,
    lamn_ref,
    lamw_ref,
    gainn_ref,
    gainw_ref,
    out_ref,
    kv,
    att,
    row_max,
    row_sum,
    acc_n,
    acc_w,
    load_sem,
    recv_sem,
    up_sem,
    first_sem,
    second_sem,
    pair_send,
    pair_recv,
    pair_ready,
):
    planes, rows, columns, tp_count = dims
    per_plane = rows * columns
    sp = lax.axis_index("sp")
    tp = lax.axis_index("tp")
    plane = sp // per_plane
    cell = sp % per_plane
    y = cell // columns
    x = cell % columns
    queries = qn_ref.shape[2]
    half_rows = queries // 2

    own = []
    begin = 0
    for index, ref in enumerate((kn_ref, vn_ref, kw_ref, vw_ref)):
        width = ref.shape[1]
        own.append(
            pltpu.make_async_copy(ref, kv.at[0, cell, :, pl.ds(begin, width)], load_sem.at[index])
        )
        begin += width
    for copy in own:
        copy.start()

    def line(axis):
        if axis == 0:
            return [((y + k) % rows) * columns + x for k in range(1, rows)]
        return [y * columns + (x + k) % columns for k in range(1, columns)]

    def crossed(other, axis):
        oy = other // columns
        ox = other % columns
        if axis == 0:
            return [((oy + k) % rows) * columns + ox for k in range(1, rows)]
        return [oy * columns + (ox + k) % columns for k in range(1, columns)]

    barrier = pltpu.get_barrier_semaphore()
    for other in line(0) + line(1):
        pl.semaphore_signal(
            barrier, inc=1, device_id={"sp": plane * per_plane + other}, device_id_type=MESH
        )
    for k in range(1, tp_count):
        pl.semaphore_signal(
            barrier, inc=1, device_id={"tp": (tp + k) % tp_count}, device_id_type=MESH
        )

    @pl.when(plane > 0)
    def _():
        pl.semaphore_signal(barrier, inc=1, device_id={"sp": sp - per_plane}, device_id_type=MESH)

    @pl.when(plane < planes - 1)
    def _():
        pl.semaphore_signal(barrier, inc=1, device_id={"sp": sp + per_plane}, device_id_type=MESH)

    below = (plane > 0).astype(jnp.int32)
    above = (plane < planes - 1).astype(jnp.int32)
    pl.semaphore_wait(barrier, rows - 1 + columns - 1 + tp_count - 1 + below + above)

    for copy in own:
        copy.wait()

    def piece(depth, block, half):
        return kv.at[depth, block, pl.ds(half * half_rows, half_rows), :]

    def remote(depth, to_depth, block, half, target, send):
        return pltpu.make_async_remote_copy(
            src_ref=piece(depth, block, half),
            dst_ref=piece(to_depth, block, half),
            send_sem=send,
            recv_sem=recv_sem.at[to_depth, block, half],
            device_id={"sp": target},
            device_id_type=MESH,
        )

    def arrived(depth, block, half):
        pltpu.make_async_remote_copy(
            src_ref=piece(depth, block, half),
            dst_ref=piece(depth, block, half),
            send_sem=up_sem.at[0, 0],
            recv_sem=recv_sem.at[depth, block, half],
            device_id={"sp": sp},
            device_id_type=MESH,
        ).wait_recv()

    def up_copies(depth):
        return [
            remote(depth, depth + 1, cell, half, sp + per_plane, up_sem.at[depth, half])
            for half in range(2)
        ]

    def direct_copies(depth):
        copies = []
        for half in range(2):
            for k, other in enumerate(line(half)):
                copies.append(
                    remote(
                        depth,
                        depth,
                        cell,
                        half,
                        plane * per_plane + other,
                        first_sem.at[depth, half, k],
                    )
                )
            for k, other in enumerate(line(1 - half)):
                copies.append(
                    remote(
                        depth,
                        depth,
                        cell,
                        half,
                        plane * per_plane + other,
                        second_sem.at[depth, half, 0, k],
                    )
                )
        return copies

    def relay_copies(depth):
        groups = []
        for half in range(2):
            for i, block in enumerate(line(half)):
                copies = [
                    remote(
                        depth,
                        depth,
                        block,
                        half,
                        plane * per_plane + other,
                        second_sem.at[depth, half, i + 1, k],
                    )
                    for k, other in enumerate(line(1 - half))
                ]
                groups.append((block, half, copies))
        return groups

    def issue(depth):
        @pl.when(plane < planes - 1)
        def _():
            for copy in up_copies(depth):
                copy.start()

        for copy in direct_copies(depth):
            copy.start()

    def relay(depth):
        for block, half, copies in relay_copies(depth):
            arrived(depth, block, half)
            for copy in copies:
                copy.start()

    def finish(depth):
        for half in range(2):
            for block in line(1 - half):
                arrived(depth, block, half)
            for first in line(half):
                for block in crossed(first, 1 - half):
                    arrived(depth, block, half)

    row_max[...] = jnp.full_like(row_max, MASKED)
    row_sum[...] = jnp.zeros_like(row_sum)
    acc_n[...] = jnp.zeros_like(acc_n)
    acc_w[...] = jnp.zeros_like(acc_w)
    heads_n = qn_ref.shape[0]
    heads_w = qw_ref.shape[1] // kw_ref.shape[1]
    width_k = kn_ref.shape[1]
    value_n = vn_ref.shape[1]
    begin_kw = width_k + value_n
    map_w = kw_ref.shape[1] // 2
    begin_vw = begin_kw + 2 * map_w
    value_w = vw_ref.shape[1]
    chunk = math.gcd(per_plane, 4)
    key_rows = chunk * queries

    def tile(query, key, value, factor, mask, state, acc, slot):
        scores = lax.dot_general(
            query, key, (((1,), (1,)), ((), ())), preferred_element_type=jnp.float32
        )
        if mask is not None:
            scores = jnp.where(mask, scores, MASKED)
        before = row_max[state][:, :1]
        now = jnp.maximum(before, jnp.max(scores, axis=1, keepdims=True))
        weights = jnp.exp2((scores - now) * factor)
        decay = jnp.exp2((before - now) * factor)
        total = row_sum[state][:, :1] * decay + jnp.sum(weights, axis=1, keepdims=True)
        acc[slot] = acc[slot] * decay + jnp.dot(
            weights.astype(jnp.bfloat16), value, preferred_element_type=jnp.float32
        )
        row_max[state] = jnp.broadcast_to(now, row_max.shape[1:])
        row_sum[state] = jnp.broadcast_to(total, row_sum.shape[1:])

    def attend(depth, masked):
        def part(at):
            def columns_of(begin, width):
                return kv[depth, pl.ds(at, chunk), :, begin : begin + width].reshape(
                    key_rows, width
                )

            mask = None
            if masked:
                query_pos = cell * queries + lax.broadcasted_iota(
                    jnp.int32, (queries, key_rows), 0
                )
                key_pos = at * queries + lax.broadcasted_iota(jnp.int32, (queries, key_rows), 1)
                mask = key_pos <= query_pos

            def narrow(head, carry):
                key = columns_of(0, width_k)
                value = columns_of(width_k, value_n)
                for which in range(2):
                    index = head * 2 + which
                    tile(
                        qn_ref[head, which],
                        key,
                        value,
                        DN**-0.5 * LOG2E,
                        mask,
                        index,
                        acc_n,
                        index,
                    )
                return carry

            def wide(head, carry):
                value = columns_of(begin_vw, value_w)
                for which in range(2):
                    index = head * 2 + which
                    tile(
                        qw_ref[:, pl.ds(pl.multiple_of(index * map_w, map_w), map_w)],
                        columns_of(begin_kw + which * map_w, map_w),
                        value,
                        DW**-0.5 * LOG2E,
                        mask,
                        2 * heads_n + index,
                        acc_w,
                        index,
                    )
                return carry

            lax.fori_loop(0, heads_n, narrow, 0)
            lax.fori_loop(0, heads_w, wide, 0)

        if per_plane == chunk:
            part(0)
        else:

            def step(at, carry):
                part(at * chunk)
                return carry

            lax.fori_loop(0, per_plane // chunk, step, 0)

    def advance(depth):
        @pl.when(depth < plane)
        def _():
            for half in range(2):
                arrived(depth + 1, cell, half)
            issue(depth + 1)

    def relay_next(depth):
        @pl.when(depth < plane)
        def _():
            relay(depth + 1)

    issue(0)
    relay(0)
    advance(0)
    finish(0)
    attend(0, True)
    relay_next(0)

    def depth_step(depth, carry):
        advance(depth)
        finish(depth)
        attend(depth, False)
        relay_next(depth)
        return carry

    lax.fori_loop(1, plane + 1, depth_step, 0)

    def close(first, second, lam, gain):
        head = first - lam * second
        scale = lax.rsqrt(jnp.mean(head * head, axis=1, keepdims=True) + EPS)
        return (head * scale * gain).astype(jnp.bfloat16)

    for head in range(heads_n):
        maps = [acc_n[2 * head + k] / row_sum[2 * head + k][:, :1] for k in range(2)]
        att[:, head * value_n : (head + 1) * value_n] = close(
            maps[0], maps[1], lamn_ref[head], gainn_ref[...]
        )
    begin_w = heads_n * value_n
    for head in range(heads_w):
        maps = [
            acc_w[2 * head + k] / row_sum[2 * (heads_n + head) + k][:, :1] for k in range(2)
        ]
        att[:, begin_w + head * value_w : begin_w + (head + 1) * value_w] = close(
            maps[0], maps[1], lamw_ref[head], gainw_ref[...]
        )

    def drain(depth, carry):
        @pl.when(plane < planes - 1)
        def _():
            for copy in up_copies(depth):
                copy.wait_send()

        for copy in direct_copies(depth):
            copy.wait_send()
        for _block, _half, copies in relay_copies(depth):
            for copy in copies:
                copy.wait_send()
        return carry

    lax.fori_loop(0, plane + 1, drain, 0)
    for k in range(1, tp_count):
        pl.semaphore_signal(
            pair_ready, inc=1, device_id={"tp": (tp + k) % tp_count}, device_id_type=MESH
        )
    pl.semaphore_wait(pair_ready, tp_count - 1)
    share = out_ref.shape[1]
    copies = []
    for k in range(1, tp_count):
        other = (tp + k) % tp_count
        copies.append(
            pltpu.make_async_remote_copy(
                src_ref=att.at[pl.ds(pl.multiple_of(other * share, share), share), :],
                dst_ref=out_ref.at[tp],
                send_sem=pair_send.at[k - 1],
                recv_sem=pair_recv.at[k - 1],
                device_id={"tp": other},
                device_id_type=MESH,
            )
        )
    for copy in copies:
        copy.start()
    out_ref[tp] = att[pl.ds(pl.multiple_of(tp * share, share), share), :]
    for copy in copies:
        copy.wait()


def attended_rows(
    sp_count,
    tp_count,
    queries_narrow,
    keys_narrow,
    values_narrow,
    queries_wide,
    keys_wide,
    values_wide,
    lambda_narrow,
    lambda_wide,
    gain_narrow,
    gain_wide,
):
    planes, rows, columns = plane_shape(sp_count)
    count = queries_narrow.shape[0]
    heads_n = queries_narrow.shape[1] // (2 * DN)
    heads_w = queries_wide.shape[1] // (2 * DW)
    maps = queries_narrow.reshape(count, heads_n, 2, DN).transpose(1, 2, 0, 3)
    padded = jnp.stack(
        [
            jnp.pad(maps[:, 0], ((0, 0), (0, 0), (0, DN))),
            jnp.pad(maps[:, 1], ((0, 0), (0, 0), (DN, 0))),
        ],
        axis=1,
    )
    width = (
        keys_narrow.shape[1] + values_narrow.shape[1] + keys_wide.shape[1] + values_wide.shape[1]
    )
    per_plane = rows * columns
    features = heads_n * VN + heads_w * VW
    longest = max(rows, columns)
    tiles = 2 * (heads_n + heads_w)
    vmem = pl.BlockSpec(memory_space=pltpu.VMEM)
    smem = pl.BlockSpec(memory_space=pltpu.SMEM)
    hbm = pl.BlockSpec(memory_space=pl.ANY)
    return pl.pallas_call(
        functools.partial(attend_kernel, (planes, rows, columns, tp_count)),
        out_shape=jax.ShapeDtypeStruct((tp_count, count // tp_count, features), jnp.bfloat16),
        in_specs=[vmem, hbm, hbm, vmem, hbm, hbm, smem, smem, vmem, vmem],
        out_specs=vmem,
        scratch_shapes=[
            pltpu.VMEM((planes, per_plane, count, width), jnp.bfloat16),
            pltpu.VMEM((count, features), jnp.bfloat16),
            pltpu.VMEM((tiles, count, 128), jnp.float32),
            pltpu.VMEM((tiles, count, 128), jnp.float32),
            pltpu.VMEM((2 * heads_n, count, VN), jnp.float32),
            pltpu.VMEM((2 * heads_w, count, VW), jnp.float32),
            pltpu.SemaphoreType.DMA((4,)),
            pltpu.SemaphoreType.DMA((planes, per_plane, 2)),
            pltpu.SemaphoreType.DMA((planes, 2)),
            pltpu.SemaphoreType.DMA((planes, 2, longest)),
            pltpu.SemaphoreType.DMA((planes, 2, longest, longest)),
            pltpu.SemaphoreType.DMA((max(1, tp_count - 1),)),
            pltpu.SemaphoreType.DMA((max(1, tp_count - 1),)),
            pltpu.SemaphoreType.REGULAR,
        ],
        compiler_params=pltpu.CompilerParams(
            collective_id=0, has_side_effects=True, vmem_limit_bytes=56 * 1024 * 1024
        ),
        name="gather_attend",
    )(
        padded,
        keys_narrow,
        values_narrow,
        queries_wide,
        keys_wide,
        values_wide,
        lambda_narrow,
        lambda_wide,
        gain_narrow.reshape(1, -1),
        gain_wide.reshape(1, -1),
    )


def run_experts(incoming, expert_gate, expert_up, expert_down, capacity):
    sources = incoming.shape[0]
    local_experts = expert_gate.shape[0]
    grouped = incoming.reshape(sources, local_experts, capacity, D)
    gate_part = jnp.einsum(
        "rjcd,jdf->rjcf", grouped, expert_gate, preferred_element_type=jnp.float32
    )
    up_part = jnp.einsum("rjcd,jdf->rjcf", grouped, expert_up, preferred_element_type=jnp.float32)
    hidden = (jax.nn.silu(gate_part) * up_part).astype(jnp.bfloat16)
    result = jnp.einsum("rjcf,jfd->rjcd", hidden, expert_down, preferred_element_type=jnp.float32)
    return result.reshape(sources, local_experts * capacity, D)


def shards(
    queries_narrow,
    keys_narrow,
    values_narrow,
    queries_wide,
    keys_wide,
    values_wide,
    lambda_narrow,
    lambda_wide,
    gain_narrow,
    gain_wide,
    out_narrow,
    out_wide,
    stream,
    gain_mix,
    gain_ffn,
    gain_post,
    shared_gate,
    shared_up,
    shared_down,
    expert_gate,
    expert_up,
    expert_down,
    expert_ids,
    route_weights,
):
    sp_count = lax.axis_size("sp")
    attended = attended_rows(
        sp_count,
        lax.axis_size("tp"),
        queries_narrow,
        keys_narrow,
        values_narrow,
        queries_wide,
        keys_wide,
        values_wide,
        lambda_narrow,
        lambda_wide,
        gain_narrow,
        gain_wide,
    )
    narrow_width = out_narrow.shape[0] // attended.shape[0]
    attended = attended.transpose(1, 0, 2)
    narrow_rows = attended[:, :, :narrow_width].reshape(attended.shape[0], -1)
    wide_rows = attended[:, :, narrow_width:].reshape(attended.shape[0], -1)
    projected = jnp.dot(narrow_rows, out_narrow, preferred_element_type=jnp.float32) + jnp.dot(
        wide_rows, out_wide, preferred_element_type=jnp.float32
    )
    mixed_rows = (stream.astype(jnp.float32) + rms_scale(projected, gain_mix)).astype(jnp.bfloat16)
    normed = rms_scale(mixed_rows.astype(jnp.float32), gain_ffn).astype(jnp.bfloat16)
    row_count = normed.shape[0]
    tp_count = lax.axis_size("tp")
    local_experts = expert_gate.shape[0]
    experts_all = local_experts * sp_count
    capacity = max(2, 3 * row_count * TOPK // (2 * experts_all))
    flat_ids = expert_ids.reshape(-1)
    onehot = (flat_ids[:, None] == jnp.arange(experts_all, dtype=jnp.int32)[None, :]).astype(
        jnp.int32
    )
    earlier = jnp.cumsum(onehot, axis=0) - onehot
    slot_rank = jnp.sum(earlier * onehot, axis=1)
    slot_index = flat_ids * capacity + slot_rank
    buffer_rows = experts_all * capacity
    selector = slot_index[None, :] == jnp.arange(buffer_rows, dtype=jnp.int32)[:, None]
    selector = jnp.any(selector.reshape(buffer_rows, row_count, TOPK), axis=2).astype(jnp.bfloat16)
    outgoing = jnp.dot(selector, normed, preferred_element_type=jnp.float32).astype(jnp.bfloat16)
    outgoing = outgoing.reshape(sp_count, local_experts * capacity, D)
    incoming = lax.all_to_all(outgoing, "sp", split_axis=0, concat_axis=0, tiled=True)
    all_rows = lax.all_gather(incoming[None], "tp", axis=0, tiled=True)
    partials = run_experts(
        all_rows.reshape(tp_count * sp_count, local_experts * capacity, D),
        expert_gate,
        expert_up,
        expert_down,
        capacity,
    )
    partials = partials.reshape(tp_count, sp_count, local_experts * capacity, D)
    own_sums = lax.psum_scatter(
        partials.astype(jnp.bfloat16), "tp", scatter_dimension=0, tiled=True
    ).astype(jnp.float32)
    returned = lax.all_to_all(
        own_sums[0].astype(jnp.bfloat16), "sp", split_axis=0, concat_axis=0, tiled=True
    )
    returned = returned.reshape(buffer_rows, D)
    picked = jnp.take(returned, slot_index, axis=0).reshape(row_count, TOPK, D)
    routed = jnp.einsum(
        "rk,rkd->rd", route_weights, picked.astype(jnp.float32), precision=lax.Precision.HIGHEST
    )
    shared_hidden = (
        jax.nn.silu(jnp.dot(normed, shared_gate, preferred_element_type=jnp.float32))
        * jnp.dot(normed, shared_up, preferred_element_type=jnp.float32)
    ).astype(jnp.bfloat16)
    shared_out = jnp.dot(shared_hidden, shared_down, preferred_element_type=jnp.float32)
    combined = shared_out + routed
    return (mixed_rows.astype(jnp.float32) + rms_scale(combined, gain_post)).astype(jnp.bfloat16)


def solution(mesh):
    return jax.shard_map(
        shards,
        mesh=mesh,
        in_specs=(
            P("sp", "tp"),
            P("sp", "tp"),
            P("sp", "tp"),
            P("sp", "tp"),
            P("sp", "tp"),
            P("sp", "tp"),
            P("tp"),
            P("tp"),
            P(),
            P(),
            P(),
            P(),
            P(("sp", "tp"), None),
            P(),
            P(),
            P(),
            P(),
            P(),
            P(),
            P("sp", None, "tp"),
            P("sp", None, "tp"),
            P("sp", "tp", None),
            P(("sp", "tp"), None),
            P(("sp", "tp"), None),
        ),
        out_specs=P(("sp", "tp"), None),
        check_vma=False,
    )
```

time: 575 us -> 329 us (0.57)
  waiting for transfers between devices: 330 us -> 100 us
  Pallas kernels: 0 us -> 46.7 us
  local copies, waits for them, and re-layouts: 38.5 us -> 18.2 us
  matrix products: 53.2 us -> 33.2 us
  other arithmetic: 14.5 us -> 5.06 us
  blocking collectives: 113 us -> 104 us
    all_gather x4 -> x0, waiting for transfers between devices: 227 us -> none  [the longest x1 64 us: shards(): lax.all_gather(keys_wide, 'sp', axis=0, tiled=True)]
    pallas_call x0 -> x1, Pallas kernels: none -> 46.7 us  [attended_rows(): pl.pallas_call(functools.partial(attend_kernel, (planes, rows, columns, t...]
    dot_general x8 -> x0, matrix products: 18.9 us -> none  [the longest x4 9.73 us: attend_block(): jnp.einsum('cgmqk,kcv->cgmqv', weights.astype(jnp.bfloat16), value_rows,...]
    all_to_all x2 -> x0, blocking collectives: 8.93 us -> none  [the longest x1 4.98 us: shards(): lax.all_to_all(narrow_out, 'tp', split_axis=0, concat_axis=1, tiled=True)]
    unnamed x36 -> x25, local copies, waits for them, and re-layouts: 9.61 us -> 2.72 us
    another operation x6 -> x3, other arithmetic: 8.15 us -> 2.04 us
  transfers between devices with their start and end apart: 7 -> 3, of which waited for: 7 -> 3; matrix products, arithmetic and copies ran while one was open for 3% -> 1% of each run, Pallas kernels for 0% -> 0%
where the time goes in v1:
time: 329 us; the launch traced here: 328 us
  blocking collectives  104 us (32%)
  waiting for transfers between devices  100 us (30%)
  Pallas kernels  46.7 us (14%)
  matrix products  33.2 us (10%)
  local copies, waits for them, and re-layouts  18.2 us (6%)
  between operations  13.6 us (4%)
  starting transfers between devices  7.31 us (2%)
  other arithmetic  5.06 us (2%)
    all_to_all x1, blocking collectives, shards(): lax.all_to_all(outgoing, 'sp', split_axis=0, concat_axis=0, tiled=True)  104 us
    all_to_all x1, waiting for transfers between devices, shards(): lax.all_to_all(own_sums[0].astype(jnp.bfloat16), 'sp', split_axis=0, conc...  67.3 us
    pallas_call x1, Pallas kernels, attended_rows(): pl.pallas_call(functools.partial(attend_kernel, (planes, rows, columns, t...  46.7 us
    all_gather x1, waiting for transfers between devices, shards(): all_rows = lax.all_gather(incoming[None], 'tp', axis=0, tiled=True)  16.9 us
    reduce_scatter x1, waiting for transfers between devices, shards(): lax.psum_scatter(partials.astype(jnp.bfloat16), 'tp', scatter_dimension=0...  16.2 us
    dot_general x1, matrix products, run_experts(): jnp.einsum('rjcf,jfd->rjcd', hidden, expert_down, preferred_element_type=...  10.1 us
    all_to_all x1, starting transfers between devices, shards(): lax.all_to_all(own_sums[0].astype(jnp.bfloat16), 'sp', split_axis=0, conc...  7.09 us
  transfers between devices with their start and end apart: 3, of which 3 were waited for; matrix products, arithmetic and copies ran while one was open for 1% of the time, Pallas kernels for 0%

profile of v1, /device:TPU:14, one launch (start us, length us, event | category | flops | bytes accessed | tf_op | source)
XLA Modules:
  0.0 328.3 jit_solution(15880384933634569378)
XLA Ops:
  6.5 0.9 copy.69
  7.7 1.1 copy.64
  8.8 0.3 copy.65
  9.3 0.8 pad_maximum_fusion.qn_ref
  10.1 46.7 %gather_attend.1 = bf16[2,128,1024]{2,1,0:T(8,128)(2,1)} custom-call(bf16[4,2,256,128]{3,2,1,0:T(8,128)(2,1)} %pad_maximum_fusion.qn_ref, bf16[256,128]{1,0:T(8,128)(2,1)} %kn_ref.1, bf16[256,128]{1,0:T(8,128)(2,1)} %vn_ref.1, bf16[256,512]{1,0:T(8,128)(2,1)} %qw_ref.1, bf16[256,256]{1,0:T(8,128)(2,1)} %kw_ref.1, bf16[256,256]{1,0:T(8,128)(2,1)} %vw_ref.1, ...), custom_call_target="tpu_custom_call" | custom-call | tf_op jit(solution)/shard_map/gather_attend/pallas_call | solution.py:440
  56.8 1.1 fusion.50
  57.9 0.2 copy.67
  58.1 0.2 copy.68
  58.3 3.1 fusion.53
  61.3 0.4 copy-done.4
  61.7 0.8 multiply_reduce_fusion.1
  62.6 0.2 copy-done.5
  62.7 0.4 fusion.24
  63.2 1.2 reduce-window.6
  64.3 0.2 slice_reduce_fusion
  64.9 0.2 fusion.14
  65.1 1.1 convolution_convert_fusion
  66.2 103.8 %all_to_all.10 = bf16[16,48,2048]{2,1,0:T(8,128)(2,1)} all-to-all(bf16[16,48,2048]{2,1,0:T(8,128)(2,1)S(1)} %bitcast.99), channel_id=1, replica_groups=mesh['sp'=16,'tp'=2] {'sp'}, dimensions={0} | all-to-all | bytes 6291456 | tf_op jit(solution)/shard_map/all_to_all | solution.py:559
  170.0 0.2 reduce-scatter.2.cloned.1.call-start
  170.3 16.9 %all-gather.3.cloned.1.call-done = bf16[32,48,2048]{2,1,0:T(8,128)(2,1)} async-done(((bf16[16,48,2048]{2,1,0:T(8,128)(2,1)}), bf16[32,48,2048]{2,1,0:T(8,128)(2,1)}) %all-gather.3.cloned.1.call-update) | async-done | bytes 6291472 | tf_op jit(solution)/shard_map/all_gather | solution.py:560
  187.2 6.4 %fusion.2 = f32[2,32,24,256]{3,2,1,0:T(8,128)} fusion(bf16[32,2,24,2048]{3,2,1,0:T(8,128)(2,1)} %bitcast.111, bf16[2,2048,256]{2,1,0:T(8,128)(2,1)} %param.43), kind=kOutput, calls=%fused_computation.4 | convolution fusion | flops 1610612736 | bytes 9961472 | tf_op jit(solution)/shard_map/rjcd,jdf->rjcf/dot_general | solution.py:483
  193.6 10.1 %convert_bitcast_fusion = bf16[32,2,24,2048]{3,2,0,1:T(8,128)(2,1)} fusion(bf16[2,256,2048]{2,1,0:T(8,128)(2,1)S(1)} %copy-done, f32[2,32,24,256]{3,2,1,0:T(8,128)} %fusion.2, bf16[2,2048,256]{2,1,0:T(8,128)(2,1)} %param.44, bf16[32,2,24,2048]{3,2,1,0:T(8,128)(2,1)} %bitcast.112), kind=kOutput, calls=%fused_computation.1 | convolution fusion | flops 3226730496 | bytes 18350080 | tf_op jit(solution)/shard_map/rjcf,jfd->rjcd/dot_general | solution.py:488
  203.7 6.6 %copy.76 = bf16[32,2,24,2048]{3,2,1,0:T(8,128)(2,1)} copy(bf16[32,2,24,2048]{3,2,0,1:T(8,128)(2,1)} %convert_bitcast_fusion) | data formatting | bytes 12582912 | tf_op jit(solution)/shard_map/convert_element_type | solution.py:570
  210.3 16.2 %reduce-scatter.2.cloned.1.call-done = bf16[1,16,48,2048]{3,2,1,0:T(8,128)(2,1)} async-done(((bf16[2,16,48,2048]{3,2,1,0:T(8,128)(2,1)}), bf16[1,16,48,2048]{3,2,1,0:T(8,128)(2,1)}) %reduce-scatter.2.cloned.1.call-update) | async-done | bytes 3145744 | tf_op jit(solution)/shard_map/reduce_scatter | solution.py:569
  226.5 7.1 %all-to-all-start.1 = ((bf16[16,48,2048]{2,1,0:T(8,128)(2,1)}), bf16[16,48,2048]{2,1,0:T(8,128)(2,1)S(1)}, u32[]{:S(2)}, u32[]{:S(2)}) async-start(bf16[16,48,2048]{2,1,0:T(8,128)(2,1)} %bitcast.100), calls=%async_computation.2 | async-start | bytes 6291456 | tf_op jit(solution)/shard_map/all_to_all | solution.py:572
  234.1 2.3 fusion.47
  236.4 67.3 %all-to-all-done.1 = bf16[16,48,2048]{2,1,0:T(8,128)(2,1)S(1)} async-done(((bf16[16,48,2048]{2,1,0:T(8,128)(2,1)}), bf16[16,48,2048]{2,1,0:T(8,128)(2,1)S(1)}, u32[]{:S(2)}, u32[]{:S(2)}) %all-to-all-start.1) | async-done | bytes 3145760 | tf_op jit(solution)/shard_map/all_to_all | solution.py:572
  303.7 3.3 %gather_fusion = bf16[512,2048]{1,0:T(8,128)(2,1)} fusion(bf16[768,2048]{1,0:T(8,128)(2,1)S(1)} %bitcast.97, s32[1024]{0:T(1024)S(1)} %pad_clamp_fusion), kind=kCustom, calls=%fused_computation | custom fusion | bytes 4196352 | tf_op jit(solution)/shard_map/jit(_take)/gather | solution.py:576
  307.0 2.7 gather.7
  309.8 4.6 %fusion.7 = f32[128,1,2048]{2,1,0:T(1,128)} fusion(f32[128,4,1]{1,2,0:T(1,128)S(1)} %copy.81, bf16[128,4,2048]{2,1,0:T(4,128)(2,1)S(1)} %gather.7, pred[128,4]{1,0:T(8,128)(4,1)S(1)} %copy.73), kind=kOutput, calls=%fused_computation.12 | convolution fusion | flops 13631488 | bytes 3148288 | tf_op jit(solution)/shard_map/rk,rkd->rd/dot_general | solution.py:577
  314.4 4.8 %multiply_reduce_fusion = (f32[128]{0:T(128)S(1)}, f32[128,2048]{1,0:T(8,128)}) fusion(f32[128,1,2048]{2,1,0:T(1,128)} %fusion.7, bf16[512,2048]{1,0:T(8,128)(2,1)} %param.42, bf16[2048,512]{1,0:T(8,128)(2,1)} %param.41, f32[128,512]{1,0:T(8,128)S(1)} %fusion.47, bf16[128,2048]{1,0:T(8,128)(2,1)S(1)} %copy-done.3, f32[2048]{0:T(1024)S(1)} %copy-done.6, ...), kind=kOutput, calls=%fused_computation.33 | convolution fusion | flops 539099008 | bytes 7087104 | tf_op jit(solution)/shard_map/dot_general | solution.py:584
  319.2 2.2 fusion.27
  (44 shorter events, 1.3 us)
Async XLA Ops:
  6.5 187.1 %copy-start = (bf16[2,256,2048]{2,1,0:T(8,128)(2,1)S(1)}, bf16[2,256,2048]{2,1,0:T(8,128)(2,1)}, u32[]{:S(2)}) copy-start(bf16[2,256,2048]{2,1,0:T(8,128)(2,1)} %param.45) | copy-start | bytes 6291460
  6.5 180.6 %all-gather.3.cloned.1.call-start = ((), (), s32[]{:S(2)}) async-start(), calls=%async_computation.4 | async-start | bytes 9437184 | tf_op jit(solution)/shard_map/all_gather | solution.py:560
  58.2 3.5 %copy-start.4 = (bf16[1024,2048]{1,0:T(8,128)(2,1)S(1)}, bf16[1024,2048]{1,0:T(8,128)(2,1)}, u32[]{:S(2)}) copy-start(bf16[1024,2048]{1,0:T(8,128)(2,1)} %param.35) | copy-start | bytes 12582916
  61.7 1.0 copy-start.5
  61.7 1.0 copy-start.8
  62.5 2.4 copy-start.7
  62.5 2.6 copy-start.6
  63.1 106.9 %copy-start.2 = (bf16[128,2048]{1,0:T(8,128)(2,1)}, bf16[128,2048]{1,0:T(8,128)(2,1)S(1)}, u32[]{:S(2)}) copy-start(bf16[128,2048]{1,0:T(8,128)(2,1)S(1)} %get-tuple-element.8) | copy-start | bytes 1572868
  170.0 56.5 %reduce-scatter.2.cloned.1.call-start = ((), (), s32[]{:S(2)}) async-start(), calls=%async_computation.3 | async-start | bytes 9437184 | tf_op jit(solution)/shard_map/reduce_scatter | solution.py:569
  226.5 7.5 %copy-start.10 = (f32[128,4]{0,1:T(4,128)S(1)}, f32[128,4]{0,1:T(4,128)}, u32[]{:S(2)}) copy-start(f32[128,4]{0,1:T(4,128)} %param.47) | copy-start | bytes 6148
  226.5 77.2 %all-to-all-start.1 = ((bf16[16,48,2048]{2,1,0:T(8,128)(2,1)}), bf16[16,48,2048]{2,1,0:T(8,128)(2,1)S(1)}, u32[]{:S(2)}, u32[]{:S(2)}) async-start(bf16[16,48,2048]{2,1,0:T(8,128)(2,1)} %bitcast.100), calls=%async_computation.2 | async-start | bytes 6291456 | tf_op jit(solution)/shard_map/all_to_all | solution.py:572
  309.8 4.6 %copy-start.3 = (bf16[128,2048]{1,0:T(8,128)(2,1)S(1)}, bf16[128,2048]{1,0:T(8,128)(2,1)}, u32[]{:S(2)}) copy-start(bf16[128,2048]{1,0:T(8,128)(2,1)} %copy-done.2) | copy-start | bytes 1572868
  314.4 4.8 %copy-start.9 = (f32[2048]{0:T(1024)S(1)}, f32[2048]{0:T(1024)}, u32[]{:S(2)}) copy-start(f32[2048]{0:T(1024)} %param.39) | copy-start | bytes 24580
  314.4 7.1 %copy-start.1 = (bf16[2,256,2048]{2,1,0:T(8,128)(2,1)S(1)}, bf16[2,256,2048]{2,1,0:T(8,128)(2,1)}, u32[]{:S(2)}) copy-start(bf16[2,256,2048]{2,1,0:T(8,128)(2,1)} %param.45) | copy-start | bytes 6291460
Sparse Core Ops, SparseCore 0:
  170.1 16.9 all-gather.2
  210.4 16.0 reduce-scatter.1

commit v2 on v1

--- a/solution.py
+++ b/solution.py
@@ -476,6 +476,423 @@
     )
 
 
+def plane_greeting(planes, rows, columns, tp_count):
+    per_plane = rows * columns
+    sp = lax.axis_index("sp")
+    tp = lax.axis_index("tp")
+    plane = sp // per_plane
+    cell = sp % per_plane
+    barrier = pltpu.get_barrier_semaphore()
+    for k in range(1, per_plane):
+        pl.semaphore_signal(
+            barrier,
+            inc=1,
+            device_id={"sp": plane * per_plane + (cell + k) % per_plane},
+            device_id_type=MESH,
+        )
+    for k in range(1, planes):
+        pl.semaphore_signal(
+            barrier,
+            inc=1,
+            device_id={"sp": (plane + k) % planes * per_plane + cell},
+            device_id_type=MESH,
+        )
+    for k in range(1, tp_count):
+        pl.semaphore_signal(
+            barrier, inc=1, device_id={"tp": (tp + k) % tp_count}, device_id_type=MESH
+        )
+    pl.semaphore_wait(barrier, per_plane - 1 + planes - 1 + tp_count - 1)
+    return plane, cell, sp, tp
+
+
+def dispatch_kernel(
+    dims,
+    group,
+    normed_ref,
+    slots_ref,
+    inbox,
+    marks,
+    held,
+    stage,
+    load_sem,
+    row_recv,
+    mark_recv,
+    row_send,
+    mark_send,
+    cell_recv,
+    cell_send,
+    pair_recv,
+    pair_send,
+):
+    planes, rows, columns, tp_count = dims
+    per_plane = rows * columns
+    sp_now = lax.axis_index("sp")
+    mine = sp_now // per_plane
+    loads = [
+        pltpu.make_async_copy(normed_ref, held.at[mine], load_sem.at[0]),
+        pltpu.make_async_copy(slots_ref, marks.at[mine], load_sem.at[1]),
+    ]
+    for copy in loads:
+        copy.start()
+    plane, cell, sp, tp = plane_greeting(planes, rows, columns, tp_count)
+    for copy in loads:
+        copy.wait()
+    padded = stage.shape[2]
+    token_count = held.shape[1]
+
+    def hops(source, way):
+        target = {"sp": (sp + per_plane * (1 if way == 0 else planes - 1)) % (planes * per_plane)}
+        return [
+            pltpu.make_async_remote_copy(
+                src_ref=marks.at[source],
+                dst_ref=marks.at[source],
+                send_sem=mark_send.at[source, way],
+                recv_sem=mark_recv.at[source],
+                device_id=target,
+                device_id_type=MESH,
+            ),
+            pltpu.make_async_remote_copy(
+                src_ref=held.at[source],
+                dst_ref=held.at[source],
+                send_sem=row_send.at[source, way],
+                recv_sem=row_recv.at[source],
+                device_id=target,
+                device_id_type=MESH,
+            ),
+        ]
+
+    def to_cell(source, k):
+        other = (cell + k) % per_plane
+        return pltpu.make_async_remote_copy(
+            src_ref=stage.at[source, other],
+            dst_ref=inbox.at[tp, source * per_plane + cell],
+            send_sem=cell_send.at[source, k],
+            recv_sem=cell_recv.at[source, (per_plane - k) % per_plane],
+            device_id={"sp": plane * per_plane + other},
+            device_id_type=MESH,
+        )
+
+    def to_pair(source, k):
+        block = inbox.at[tp, pl.ds(source * per_plane, per_plane)]
+        return pltpu.make_async_remote_copy(
+            src_ref=block,
+            dst_ref=block,
+            send_sem=pair_send.at[source, k - 1],
+            recv_sem=pair_recv.at[source, k - 1],
+            device_id={"tp": (tp + k) % tp_count},
+            device_id_type=MESH,
+        )
+
+    steps = [(0, 0)] + [(d, way) for d in range(1, planes) for way in range(2)]
+
+    def of_step(d, way):
+        source = plane - d if way == 0 else plane + d
+        exists = source >= 0 if way == 0 else source < planes
+        return source, exists
+
+    def onward(source, d, way, act):
+        for side in ((0, 1) if d == 0 else (way,)):
+
+            @pl.when(plane < planes - 1 if side == 0 else plane > 0)
+            def _(side=side):
+                for copy in hops(source, side):
+                    act(copy)
+
+    def start(copy):
+        copy.start()
+
+    def wait_send(copy):
+        copy.wait_send()
+
+    def body(d, way):
+        source, exists = of_step(d, way)
+
+        @pl.when(exists)
+        def _():
+            if d > 0:
+                for copy in hops(source, way):
+                    copy.wait_recv()
+            onward(source, d, way, start)
+            tokens = held[source]
+            slots = marks[source]
+            row = lax.broadcasted_iota(jnp.int32, (padded, token_count), 0)
+            for k in list(range(1, per_plane)) + [0]:
+                other = (cell + k) % per_plane
+                base = (plane * per_plane + other) * group
+                wanted = jnp.where(row < group, row + base, -1).astype(jnp.float32)
+                hit = slots[0:1, :] == wanted
+                for choice in range(1, TOPK):
+                    hit = hit | (slots[choice : choice + 1, :] == wanted)
+                chosen = jnp.dot(
+                    jnp.where(hit, 1.0, 0.0).astype(jnp.bfloat16),
+                    tokens,
+                    preferred_element_type=jnp.float32,
+                ).astype(jnp.bfloat16)
+                if k == 0:
+                    inbox[tp, source * per_plane + cell] = chosen
+                else:
+                    stage[source, other] = chosen
+            for k in range(1, per_plane):
+                to_cell(source, k).start()
+
+    def finish(d, way):
+        source, exists = of_step(d, way)
+
+        @pl.when(exists)
+        def _():
+            for k in range(1, per_plane):
+                pltpu.make_async_remote_copy(
+                    src_ref=stage.at[source, cell],
+                    dst_ref=inbox.at[tp, source * per_plane + (cell + k) % per_plane],
+                    send_sem=cell_send.at[source, k],
+                    recv_sem=cell_recv.at[source, k],
+                    device_id={"sp": sp},
+                    device_id_type=MESH,
+                ).wait_recv()
+            for k in range(1, tp_count):
+                to_pair(source, k).start()
+
+    for index, step in enumerate(steps):
+        body(*step)
+        if index > 0:
+            finish(*steps[index - 1])
+    finish(*steps[-1])
+    for d, way in steps:
+        source, exists = of_step(d, way)
+
+        @pl.when(exists)
+        def _(source=source, d=d, way=way):
+            onward(source, d, way, wait_send)
+            for k in range(1, per_plane):
+                to_cell(source, k).wait_send()
+            for k in range(1, tp_count):
+                to_pair(source, k).wait()
+
+
+def dispatched_rows(dims, group, normed, slot_index, route_weights):
+    planes, rows, columns, tp_count = dims
+    per_plane = rows * columns
+    token_count, width = normed.shape
+    padded = -(-group // 16) * 16
+    slots = slot_index.reshape(token_count, TOPK).astype(jnp.float32)
+    slots = jnp.concatenate([slots, route_weights], axis=1).T
+    hbm = pl.BlockSpec(memory_space=pl.ANY)
+    dma = pltpu.SemaphoreType.DMA
+    return pl.pallas_call(
+        functools.partial(dispatch_kernel, dims, group),
+        out_shape=[
+            jax.ShapeDtypeStruct((tp_count, planes * per_plane, padded, width), jnp.bfloat16),
+            jax.ShapeDtypeStruct((planes, 2 * TOPK, token_count), jnp.float32),
+        ],
+        in_specs=[hbm, hbm],
+        out_specs=[pl.BlockSpec(memory_space=pltpu.VMEM)] * 2,
+        scratch_shapes=[
+            pltpu.VMEM((planes, token_count, width), jnp.bfloat16),
+            pltpu.VMEM((planes, per_plane, padded, width), jnp.bfloat16),
+            dma((2,)),
+            dma((planes,)),
+            dma((planes,)),
+            dma((planes, 2)),
+            dma((planes, 2)),
+            dma((planes, per_plane)),
+            dma((planes, per_plane)),
+            dma((planes, max(1, tp_count - 1))),
+            dma((planes, max(1, tp_count - 1))),
+        ],
+        compiler_params=pltpu.CompilerParams(
+            collective_id=1, has_side_effects=True, vmem_limit_bytes=56 * 1024 * 1024
+        ),
+        name="dispatch",
+    )(normed, slots)
+
+
+def combine_kernel(
+    dims,
+    group,
+    parts_ref,
+    marks_ref,
+    out_ref,
+    mine,
+    theirs,
+    stage,
+    back,
+    leaving,
+    landed,
+    load_sem,
+    pair_recv,
+    pair_send,
+    cell_recv,
+    cell_send,
+    far_recv,
+    far_send,
+):
+    planes, rows, columns, tp_count = dims
+    per_plane = rows * columns
+    plane, cell, sp, tp = plane_greeting(planes, rows, columns, tp_count)
+    padded = stage.shape[2]
+    token_count = out_ref.shape[0]
+    order = list(range(1, planes)) + [0]
+
+    def source_of(step):
+        return (plane + step) % planes
+
+    def load(step):
+        source = source_of(step)
+        return pltpu.make_async_copy(
+            parts_ref.at[tp, pl.ds(source * per_plane, per_plane)],
+            mine.at[source],
+            load_sem.at[step],
+        )
+
+    def to_pair(step, k):
+        source = source_of(step)
+        other = (tp + k) % tp_count
+        return pltpu.make_async_remote_copy(
+            src_ref=parts_ref.at[other, pl.ds(source * per_plane, per_plane)],
+            dst_ref=theirs.at[k - 1, source],
+            send_sem=pair_send.at[step, k - 1],
+            recv_sem=pair_recv.at[step, k - 1],
+            device_id={"tp": other},
+            device_id_type=MESH,
+        )
+
+    def to_cell(step, k):
+        source = source_of(step)
+        other = (cell + k) % per_plane
+        return pltpu.make_async_remote_copy(
+            src_ref=stage.at[source, other],
+            dst_ref=back.at[source, cell],
+            send_sem=cell_send.at[step, k],
+            recv_sem=cell_recv.at[step, (per_plane - k) % per_plane],
+            device_id={"sp": plane * per_plane + other},
+            device_id_type=MESH,
+        )
+
+    def to_far(step):
+        return pltpu.make_async_remote_copy(
+            src_ref=leaving.at[step],
+            dst_ref=landed.at[step],
+            send_sem=far_send.at[step],
+            recv_sem=far_recv.at[step],
+            device_id={"sp": source_of(step) * per_plane + cell},
+            device_id_type=MESH,
+        )
+
+    for step in order:
+        load(step).start()
+        for k in range(1, tp_count):
+            to_pair(step, k).start()
+
+    def body(step):
+        source = source_of(step)
+        load(step).wait()
+        for k in range(1, tp_count):
+            to_pair(step, k).wait_recv()
+        for k in list(range(1, per_plane)) + [0]:
+            other = (cell + k) % per_plane
+            total = mine[source, other].astype(jnp.float32)
+            for i in range(tp_count - 1):
+                total += theirs[i, source, other].astype(jnp.float32)
+            if k == 0:
+                back[source, cell] = total.astype(jnp.bfloat16)
+            else:
+                stage[source, other] = total.astype(jnp.bfloat16)
+        for k in range(1, per_plane):
+            to_cell(step, k).start()
+
+    def finish(step):
+        source = source_of(step)
+        for k in range(1, per_plane):
+            pltpu.make_async_remote_copy(
+                src_ref=stage.at[source, cell],
+                dst_ref=back.at[source, (cell + k) % per_plane],
+                send_sem=cell_send.at[step, k],
+                recv_sem=cell_recv.at[step, k],
+                device_id={"sp": sp},
+                device_id_type=MESH,
+            ).wait_recv()
+        marks = marks_ref[source]
+        row = lax.broadcasted_iota(jnp.int32, (per_plane * padded, token_count), 0)
+        block = lax.div(row, padded)
+        inner = row - block * padded
+        wanted = jnp.where(
+            inner < group, inner + (plane * per_plane + block) * group, -1
+        ).astype(jnp.float32)
+        share = jnp.zeros(wanted.shape, jnp.float32)
+        for choice in range(TOPK):
+            share += jnp.where(
+                marks[choice : choice + 1, :] == wanted,
+                marks[TOPK + choice : TOPK + choice + 1, :],
+                0.0,
+            )
+        high = share.astype(jnp.bfloat16)
+        low = (share - high.astype(jnp.float32)).astype(jnp.bfloat16)
+        both = jnp.concatenate([high, low], axis=1)
+        for at in range(0, out_ref.shape[1], 512):
+            values = back[source, :, :, at : at + 512].reshape(per_plane * padded, 512)
+            pieces = lax.dot_general(
+                both, values, (((0,), (0,)), ((), ())), preferred_element_type=jnp.float32
+            )
+            total = pieces[:token_count] + pieces[token_count:]
+            if step == 0:
+                out_ref[:, at : at + 512] = total
+            else:
+                leaving[step, :, at : at + 512] = total.astype(jnp.bfloat16)
+        if step > 0:
+            to_far(step).start()
+
+    for index, step in enumerate(order):
+        body(step)
+        if index > 0:
+            finish(order[index - 1])
+    finish(order[-1])
+    for step in range(1, planes):
+        to_far(step).wait_recv()
+        out_ref[...] += landed[step].astype(jnp.float32)
+    for step in order:
+        for k in range(1, tp_count):
+            to_pair(step, k).wait_send()
+        for k in range(1, per_plane):
+            to_cell(step, k).wait_send()
+        if step > 0:
+            to_far(step).wait_send()
+
+
+def combined_rows(dims, group, parts, marks):
+    planes, rows, columns, tp_count = dims
+    per_plane = rows * columns
+    padded, width = parts.shape[2:]
+    token_count = marks.shape[2]
+    dma = pltpu.SemaphoreType.DMA
+    block = (planes, per_plane, padded, width)
+    pairs = max(1, tp_count - 1)
+    return pl.pallas_call(
+        functools.partial(combine_kernel, dims, group),
+        out_shape=jax.ShapeDtypeStruct((token_count, width), jnp.float32),
+        in_specs=[pl.BlockSpec(memory_space=pl.ANY), pl.BlockSpec(memory_space=pltpu.VMEM)],
+        out_specs=pl.BlockSpec(memory_space=pltpu.VMEM),
+        scratch_shapes=[
+            pltpu.VMEM(block, jnp.bfloat16),
+            pltpu.VMEM((pairs,) + block, jnp.bfloat16),
+            pltpu.VMEM(block, jnp.bfloat16),
+            pltpu.VMEM(block, jnp.bfloat16),
+            pltpu.VMEM((planes, token_count, width), jnp.bfloat16),
+            pltpu.VMEM((planes, token_count, width), jnp.bfloat16),
+            dma((planes,)),
+            dma((planes, pairs)),
+            dma((planes, pairs)),
+            dma((planes, per_plane)),
+            dma((planes, per_plane)),
+            dma((planes,)),
+            dma((planes,)),
+        ],
+        compiler_params=pltpu.CompilerParams(
+            collective_id=2, has_side_effects=True, vmem_limit_bytes=56 * 1024 * 1024
+        ),
+        name="combine",
+    )(parts, marks)
+
+
 def run_experts(incoming, expert_gate, expert_up, expert_down, capacity):
     sources = incoming.shape[0]
     local_experts = expert_gate.shape[0]
@@ -551,32 +968,21 @@
     earlier = jnp.cumsum(onehot, axis=0) - onehot
     slot_rank = jnp.sum(earlier * onehot, axis=1)
     slot_index = flat_ids * capacity + slot_rank
-    buffer_rows = experts_all * capacity
-    selector = slot_index[None, :] == jnp.arange(buffer_rows, dtype=jnp.int32)[:, None]
-    selector = jnp.any(selector.reshape(buffer_rows, row_count, TOPK), axis=2).astype(jnp.bfloat16)
-    outgoing = jnp.dot(selector, normed, preferred_element_type=jnp.float32).astype(jnp.bfloat16)
-    outgoing = outgoing.reshape(sp_count, local_experts * capacity, D)
-    incoming = lax.all_to_all(outgoing, "sp", split_axis=0, concat_axis=0, tiled=True)
-    all_rows = lax.all_gather(incoming[None], "tp", axis=0, tiled=True)
+    group = local_experts * capacity
+    dims = plane_shape(sp_count) + (tp_count,)
+    all_rows, marks = dispatched_rows(dims, group, normed, slot_index, route_weights)
+    padded = all_rows.shape[2]
     partials = run_experts(
-        all_rows.reshape(tp_count * sp_count, local_experts * capacity, D),
+        all_rows[:, :, :group].reshape(tp_count * sp_count, group, D),
         expert_gate,
         expert_up,
         expert_down,
         capacity,
     )
-    partials = partials.reshape(tp_count, sp_count, local_experts * capacity, D)
-    own_sums = lax.psum_scatter(
-        partials.astype(jnp.bfloat16), "tp", scatter_dimension=0, tiled=True
-    ).astype(jnp.float32)
-    returned = lax.all_to_all(
-        own_sums[0].astype(jnp.bfloat16), "sp", split_axis=0, concat_axis=0, tiled=True
-    )
-    returned = returned.reshape(buffer_rows, D)
-    picked = jnp.take(returned, slot_index, axis=0).reshape(row_count, TOPK, D)
-    routed = jnp.einsum(
-        "rk,rkd->rd", route_weights, picked.astype(jnp.float32), precision=lax.Precision.HIGHEST
-    )
+    partials = partials.astype(jnp.bfloat16).reshape(tp_count, sp_count, group, D)
+    if padded > group:
+        partials = jnp.pad(partials, ((0, 0), (0, 0), (0, padded - group), (0, 0)))
+    routed = combined_rows(dims, group, partials, marks)
     shared_hidden = (
         jax.nn.silu(jnp.dot(normed, shared_gate, preferred_element_type=jnp.float32))
         * jnp.dot(normed, shared_up, preferred_element_type=jnp.float32)

time: 329 us -> 249 us (0.76)
  Pallas kernels: 46.7 us -> 202 us
  blocking collectives: 104 us -> 0 us
  waiting for transfers between devices: 100 us -> 0 us
  between operations: 13.6 us -> 0.18 us
  starting transfers between devices: 7.31 us -> 0 us
  local copies, waits for them, and re-layouts: 18.2 us -> 12 us
  matrix products: 33.2 us -> 27.5 us
    pallas_call x0 -> x2, Pallas kernels: none -> 155 us  [the longest x1 77.6 us: combined_rows(): pl.pallas_call(functools.partial(combine_kernel, dims, group), out_shape=...]
    all_to_all x1 -> x0, blocking collectives: 104 us -> none  [shards(): lax.all_to_all(outgoing, 'sp', split_axis=0, concat_axis=0, tiled=True)]
    all_to_all x1 -> x0, waiting for transfers between devices: 67.3 us -> none  [shards(): lax.all_to_all(own_sums[0].astype(jnp.bfloat16), 'sp', split_axis=0, conc...]
    all_gather x1 -> x0, waiting for transfers between devices: 16.9 us -> none  [shards(): all_rows = lax.all_gather(incoming[None], 'tp', axis=0, tiled=True)]
    reduce_scatter x1 -> x0, waiting for transfers between devices: 16.2 us -> none  [shards(): lax.psum_scatter(partials.astype(jnp.bfloat16), 'tp', scatter_dimension=0...]
    all_to_all x1 -> x0, starting transfers between devices: 7.09 us -> none  [shards(): lax.all_to_all(own_sums[0].astype(jnp.bfloat16), 'sp', split_axis=0, conc...]
    gather x2 -> x0, local copies, waits for them, and re-layouts: 6.07 us -> none  [shards(): picked = jnp.take(returned, slot_index, axis=0).reshape(row_count, TOPK, D)]
    dot_general x2 -> x0, matrix products: 5.65 us -> none  [the longest x1 4.59 us: shards(): jnp.einsum('rk,rkd->rd', route_weights, picked.astype(jnp.float32), preci...]
  transfers between devices with their start and end apart: 3 -> 0, of which waited for: 3 -> 0; matrix products, arithmetic and copies ran while one was open for 1% -> 0% of each run, Pallas kernels for 0% -> 0%
where the time goes in v2:
time: 249 us; the launch traced here: 248 us
  Pallas kernels  202 us (81%)
  matrix products  27.5 us (11%)
  local copies, waits for them, and re-layouts  12 us (5%)
  other arithmetic  6.41 us (3%)
    pallas_call x1, Pallas kernels, combined_rows(): pl.pallas_call(functools.partial(combine_kernel, dims, group), out_shape=...  77.6 us
    pallas_call x1, Pallas kernels, dispatched_rows(): pl.pallas_call(functools.partial(dispatch_kernel, dims, group), out_shape...  77.4 us
    pallas_call x1, Pallas kernels, attended_rows(): pl.pallas_call(functools.partial(attend_kernel, (planes, rows, columns, t...  46.7 us
    dot_general x1, matrix products, run_experts(): jnp.einsum('rjcf,jfd->rjcd', hidden, expert_down, preferred_element_type=...  10.1 us
    convert_element_type x1, local copies, waits for them, and re-layouts, shards(): partials.astype(jnp.bfloat16).reshape(tp_count, sp_count, group, D)  6.57 us
    dot_general x1, matrix products, run_experts(): jnp.einsum('rjcd,jdf->rjcf', grouped, expert_gate, preferred_element_type...  6.43 us

profile of v2, /device:TPU:14, one launch (start us, length us, event | category | flops | bytes accessed | tf_op | source)
XLA Modules:
  0.0 247.8 jit_solution(2443415135240648023)
XLA Ops:
  0.0 1.2 copy.28
  1.2 0.3 copy.29
  1.6 0.2 pad_bitcast_fusion
  1.7 0.8 pad_maximum_fusion.qn_ref
  2.6 46.7 %gather_attend.1 = bf16[2,128,1024]{2,1,0:T(8,128)(2,1)} custom-call(bf16[4,2,256,128]{3,2,1,0:T(8,128)(2,1)} %pad_maximum_fusion.qn_ref, bf16[256,128]{1,0:T(8,128)(2,1)} %kn_ref.1, bf16[256,128]{1,0:T(8,128)(2,1)} %vn_ref.1, bf16[256,512]{1,0:T(8,128)(2,1)} %qw_ref.1, bf16[256,256]{1,0:T(8,128)(2,1)} %kw_ref.1, bf16[256,256]{1,0:T(8,128)(2,1)} %vw_ref.1, ...), custom_call_target="tpu_custom_call" | custom-call | tf_op jit(solution)/shard_map/gather_attend/pallas_call | solution.py:440
  49.3 1.1 fusion.37
  50.4 0.8 copy.31
  51.2 3.0 %fusion.38 = f32[128,2048]{1,0:T(8,128)S(1)} fusion(bf16[128,1024]{0,1:T(8,128)(2,1)} %bitcast.96, bf16[1024,2048]{1,0:T(8,128)(2,1)} %param.34), kind=kOutput, calls=%fused_computation.58 | convolution fusion | flops 536870912 | bytes 5505024 | tf_op jit(solution)/shard_map/dot_general | solution.py:954
  54.2 0.8 copy.32
  55.1 3.1 %multiply_reduce_fusion.1 = (f32[128]{0:T(128)S(1)}, f32[128,2048]{1,0:T(8,128)S(1)}) fusion(f32[128,2048]{1,0:T(8,128)S(1)} %fusion.38, bf16[128,1024]{0,1:T(8,128)(2,1)} %bitcast.95, bf16[1024,2048]{1,0:T(8,128)(2,1)} %param.35), kind=kOutput, calls=%fused_computation.28 | convolution fusion | flops 537657216 | bytes 6554112 | tf_op jit(solution)/shard_map/dot_general | solution.py:954
  58.2 0.0 copy-start.5
  58.2 0.0 copy-start.7
  58.3 0.4 fusion.20
  58.7 0.3 copy-done.5
  58.9 1.0 fusion.22.normed_ref
  59.9 0.1 copy.33
  60.0 0.1 eq.29
  60.1 1.2 reduce-window.6
  61.3 0.2 slice_reduce_fusion
  61.6 0.1 eq.25
  61.7 0.1 fusion.33
  61.8 0.1 reduce_sum.41
  61.9 0.1 copy.36
  62.0 0.6 maximum_bitcast_fusion.slots_ref
  62.6 77.4 %dispatch.1 = (bf16[2,16,48,2048]{3,2,1,0:T(8,128)(2,1)}, f32[4,8,128]{2,1,0:T(8,128)}) custom-call(bf16[128,2048]{1,0:T(8,128)(2,1)} %fusion.22.normed_ref, f32[8,128]{1,0:T(8,128)} %maximum_bitcast_fusion.slots_ref), custom_call_target="tpu_custom_call" | custom-call | tf_op jit(solution)/shard_map/dispatch/pallas_call | solution.py:681
  140.0 6.4 %fusion.2 = f32[2,32,24,256]{3,2,1,0:T(8,128)} fusion(bf16[32,2,24,2048]{3,2,1,0:T(8,128)(2,1)} %bitcast.99, bf16[2,2048,256]{2,1,0:T(8,128)(2,1)} %param.43), kind=kOutput, calls=%fused_computation.3 | convolution fusion | flops 1610612736 | bytes 9961472 | tf_op jit(solution)/shard_map/rjcd,jdf->rjcf/dot_general | solution.py:900
  146.4 10.1 %convert_bitcast_fusion = bf16[32,2,24,2048]{3,2,0,1:T(8,128)(2,1)} fusion(bf16[2,256,2048]{2,1,0:T(8,128)(2,1)S(1)} %copy-done, f32[2,32,24,256]{3,2,1,0:T(8,128)} %fusion.2, bf16[2,2048,256]{2,1,0:T(8,128)(2,1)} %param.44, bf16[32,2,24,2048]{3,2,1,0:T(8,128)(2,1)} %bitcast.100), kind=kOutput, calls=%fused_computation | convolution fusion | flops 3226730496 | bytes 18350080 | tf_op jit(solution)/shard_map/rjcf,jfd->rjcd/dot_general | solution.py:905
  156.5 6.6 %copy.38 = bf16[32,2,24,2048]{3,2,1,0:T(8,128)(2,1)} copy(bf16[32,2,24,2048]{3,2,0,1:T(8,128)(2,1)} %convert_bitcast_fusion) | data formatting | bytes 12582912 | tf_op jit(solution)/shard_map/convert_element_type | solution.py:982
  163.1 77.6 %combine.1 = f32[128,2048]{1,0:T(8,128)} custom-call(bf16[2,16,48,2048]{3,2,1,0:T(8,128)(2,1)} %bitcast.91, f32[4,8,128]{2,1,0:T(8,128)} %get-tuple-element.8.marks_ref), custom_call_target="tpu_custom_call" | custom-call | tf_op jit(solution)/shard_map/combine/pallas_call | solution.py:869
  240.7 0.4 fusion.39
  241.2 4.4 %multiply_reduce_fusion = (f32[128]{0:T(128)S(1)}, f32[128,2048]{1,0:T(8,128)}) fusion(f32[128,2048]{1,0:T(8,128)} %combine.1, bf16[512,2048]{1,0:T(8,128)(2,1)} %param.42, bf16[128,2048]{1,0:T(8,128)(2,1)S(1)} %copy-done.1, bf16[2048,512]{1,0:T(8,128)(2,1)} %param.41, f32[128,512]{1,0:T(8,128)S(1)} %fusion.39), kind=kOutput, calls=%fused_computation.26 | convolution fusion | flops 538050432 | bytes 7078400 | tf_op jit(solution)/shard_map/dot_general | solution.py:990
  245.6 2.2 fusion.23
  (23 shorter events, 0.2 us)
Async XLA Ops:
  0.0 146.4 %copy-start = (bf16[2,256,2048]{2,1,0:T(8,128)(2,1)S(1)}, bf16[2,256,2048]{2,1,0:T(8,128)(2,1)}, u32[]{:S(2)}) copy-start(bf16[2,256,2048]{2,1,0:T(8,128)(2,1)} %param.45) | copy-start | bytes 6291460
  55.1 3.2 %copy-start.3 = (bf16[128,2048]{1,0:T(8,128)(2,1)S(1)}, bf16[128,2048]{1,0:T(8,128)(2,1)}, u32[]{:S(2)}) copy-start(bf16[128,2048]{1,0:T(8,128)(2,1)} %param.36) | copy-start | bytes 1572868
  55.1 3.2 %copy-start.4 = (f32[2048]{0:T(1024)S(1)}, f32[2048]{0:T(1024)}, u32[]{:S(2)}) copy-start(f32[2048]{0:T(1024)} %param.37) | copy-start | bytes 24580
  58.2 0.7 copy-start.5
  58.2 1.7 copy-start.7
  58.2 3.7 %copy-start.8 = (f32[128,4]{0,1:T(4,128)S(1)}, f32[128,4]{0,1:T(4,128)}, u32[]{:S(2)}) copy-start(f32[128,4]{0,1:T(4,128)} %param.47) | copy-start | bytes 6148
  163.1 77.6 %copy-start.1 = (bf16[128,2048]{1,0:T(8,128)(2,1)S(1)}, bf16[128,2048]{1,0:T(8,128)(2,1)}, u32[]{:S(2)}) copy-start(bf16[128,2048]{1,0:T(8,128)(2,1)} %fusion.22.normed_ref) | copy-start | bytes 1572868
  163.1 77.6 %copy-start.2 = (bf16[2048,512]{1,0:T(8,128)(2,1)S(1)}, bf16[2048,512]{1,0:T(8,128)(2,1)}, u32[]{:S(2)}) copy-start(bf16[2048,512]{1,0:T(8,128)(2,1)} %param.40) | copy-start | bytes 6291460
  241.2 4.4 %copy-start.6 = (f32[2048]{0:T(1024)S(1)}, f32[2048]{0:T(1024)}, u32[]{:S(2)}) copy-start(f32[2048]{0:T(1024)} %param.39) | copy-start | bytes 24580

commit v3 on v2

--- a/solution.py
+++ b/solution.py
@@ -902,7 +902,15 @@
     )
     up_part = jnp.einsum("rjcd,jdf->rjcf", grouped, expert_up, preferred_element_type=jnp.float32)
     hidden = (jax.nn.silu(gate_part) * up_part).astype(jnp.bfloat16)
-    result = jnp.einsum("rjcf,jfd->rjcd", hidden, expert_down, preferred_element_type=jnp.float32)
+    result = jnp.stack(
+        [
+            jnp.einsum(
+                "rcf,fd->rcd", hidden[:, j], expert_down[j], preferred_element_type=jnp.float32
+            ).astype(jnp.bfloat16)
+            for j in range(local_experts)
+        ],
+        axis=1,
+    )
     return result.reshape(sources, local_experts * capacity, D)
 
 

time: 249 us -> 239 us (0.960)
  matrix products: 27.5 us -> 19.9 us
  local copies, waits for them, and re-layouts: 12 us -> 9.16 us
    convert_element_type x1 -> x0, local copies, waits for them, and re-layouts: 6.57 us -> none  [shards(): partials.astype(jnp.bfloat16).reshape(tp_count, sp_count, group, D)]
    dot_general x1 -> x3, matrix products: 10.1 us -> 4.13 us  [the longest x1 2.16 us: run_experts(): jnp.einsum('rjcd,jdf->rjcf', grouped, expert_up, preferred_element_type=j...]
    another operation x1 -> x2, local copies, waits for them, and re-layouts: 0.01 us -> 3.24 us  [the longest x1 3.24 us: run_experts(): jnp.stack([jnp.einsum('rcf,fd->rcd', hidden[:, j], expert_down[j], prefer...]
where the time goes in v3:
time: 239 us; the launch traced here: 238 us
  Pallas kernels  202 us (85%)
  matrix products  19.9 us (8%)
  local copies, waits for them, and re-layouts  9.16 us (4%)
  other arithmetic  6.99 us (3%)
    pallas_call x1, Pallas kernels, combined_rows(): pl.pallas_call(functools.partial(combine_kernel, dims, group), out_shape=...  77.6 us
    pallas_call x1, Pallas kernels, dispatched_rows(): pl.pallas_call(functools.partial(dispatch_kernel, dims, group), out_shape...  77.4 us
    pallas_call x1, Pallas kernels, attended_rows(): pl.pallas_call(functools.partial(attend_kernel, (planes, rows, columns, t...  46.7 us

profile of v3, /device:TPU:14, one launch (start us, length us, event | category | flops | bytes accessed | tf_op | source)
XLA Modules:
  0.0 237.9 jit_solution(8839516690784269144)
XLA Ops:
  0.0 1.2 copy.29
  1.2 0.3 copy.30
  1.6 0.2 pad_bitcast_fusion
  1.7 0.8 pad_maximum_fusion.1.qn_ref
  2.6 46.7 %gather_attend.1 = bf16[2,128,1024]{2,1,0:T(8,128)(2,1)} custom-call(bf16[4,2,256,128]{3,2,1,0:T(8,128)(2,1)} %pad_maximum_fusion.1.qn_ref, bf16[256,128]{1,0:T(8,128)(2,1)} %kn_ref.1, bf16[256,128]{1,0:T(8,128)(2,1)} %vn_ref.1, bf16[256,512]{1,0:T(8,128)(2,1)} %qw_ref.1, bf16[256,256]{1,0:T(8,128)(2,1)} %kw_ref.1, bf16[256,256]{1,0:T(8,128)(2,1)} %vw_ref.1, ...), custom_call_target="tpu_custom_call" | custom-call | tf_op jit(solution)/shard_map/gather_attend/pallas_call | solution.py:440
  49.3 1.1 fusion.36
  50.4 0.8 copy.32
  51.2 3.0 %fusion.37 = f32[128,2048]{1,0:T(8,128)S(1)} fusion(bf16[128,1024]{0,1:T(8,128)(2,1)} %bitcast.101, bf16[1024,2048]{1,0:T(8,128)(2,1)} %param.34), kind=kOutput, calls=%fused_computation.65 | convolution fusion | flops 536870912 | bytes 5505024 | tf_op jit(solution)/shard_map/dot_general | solution.py:962
  54.2 0.8 copy.33
  55.1 3.1 %multiply_reduce_fusion.1 = (f32[128]{0:T(128)S(1)}, f32[128,2048]{1,0:T(8,128)S(1)}) fusion(f32[128,2048]{1,0:T(8,128)S(1)} %fusion.37, bf16[128,1024]{0,1:T(8,128)(2,1)} %bitcast.100, bf16[1024,2048]{1,0:T(8,128)(2,1)} %param.35), kind=kOutput, calls=%fused_computation.35 | convolution fusion | flops 537657216 | bytes 6554112 | tf_op jit(solution)/shard_map/dot_general | solution.py:962
  58.3 0.4 fusion.17
  58.7 0.3 copy-done.6
  58.9 1.0 fusion.19.normed_ref
  59.9 0.1 copy.34
  60.0 0.1 eq.29
  60.1 1.2 reduce-window.6
  61.3 0.2 slice_reduce_fusion
  61.6 0.1 eq.25
  61.8 0.1 reduce_sum.41
  62.0 0.6 maximum_bitcast_fusion.slots_ref
  62.6 77.4 %dispatch.1 = (bf16[2,16,48,2048]{3,2,1,0:T(8,128)(2,1)}, f32[4,8,128]{2,1,0:T(8,128)}) custom-call(bf16[128,2048]{1,0:T(8,128)(2,1)} %fusion.19.normed_ref, f32[8,128]{1,0:T(8,128)} %maximum_bitcast_fusion.slots_ref), custom_call_target="tpu_custom_call" | custom-call | tf_op jit(solution)/shard_map/dispatch/pallas_call | solution.py:681
  140.0 4.8 %fusion.2 = f32[2,32,24,256]{3,2,1,0:T(8,128)S(1)} fusion(bf16[32,2,24,2048]{3,2,1,0:T(8,128)(2,1)} %bitcast.104, bf16[2,2048,256]{2,1,0:T(8,128)(2,1)S(1)} %copy-done), kind=kOutput, calls=%fused_computation.3 | convolution fusion | flops 1610612736 | bytes 9961472 | tf_op jit(solution)/shard_map/rjcd,jdf->rjcf/dot_general | solution.py:900
  144.8 0.4 copy-done.11
  145.2 2.2 fusion.8
  147.4 1.0 fusion.4
  148.4 1.0 fusion.5
  149.4 0.6 pad_maximum_fusion
  150.0 3.2 %copy.40 = bf16[32,2,24,2048]{3,2,1,0:T(8,128)(2,1)} copy(bf16[32,2,24,2048]{3,2,0,1:T(8,128)(2,1)S(1)} %pad_maximum_fusion) | data formatting | bytes 12582912 | tf_op jit(solution)/shard_map/stack | solution.py:905
  153.2 77.6 %combine.1 = f32[128,2048]{1,0:T(8,128)} custom-call(bf16[2,16,48,2048]{3,2,1,0:T(8,128)(2,1)} %bitcast.96, f32[4,8,128]{2,1,0:T(8,128)} %get-tuple-element.8.marks_ref), custom_call_target="tpu_custom_call" | custom-call | tf_op jit(solution)/shard_map/combine/pallas_call | solution.py:869
  230.8 0.4 fusion.38
  231.3 4.4 %multiply_reduce_fusion = (f32[128]{0:T(128)S(1)}, f32[128,2048]{1,0:T(8,128)}) fusion(f32[128,2048]{1,0:T(8,128)} %combine.1, bf16[512,2048]{1,0:T(8,128)(2,1)} %param.42, bf16[128,2048]{1,0:T(8,128)(2,1)S(1)} %copy-done.1, bf16[2048,512]{1,0:T(8,128)(2,1)} %param.41, f32[128,512]{1,0:T(8,128)S(1)} %fusion.38), kind=kOutput, calls=%fused_computation.31 | convolution fusion | flops 538050432 | bytes 7078400 | tf_op jit(solution)/shard_map/dot_general | solution.py:998
  235.7 2.2 fusion.20
  (32 shorter events, 0.3 us)
Async XLA Ops:
  0.0 140.0 %copy-start = (bf16[2,2048,256]{2,1,0:T(8,128)(2,1)S(1)}, bf16[2,2048,256]{2,1,0:T(8,128)(2,1)}, u32[]{:S(2)}) copy-start(bf16[2,2048,256]{2,1,0:T(8,128)(2,1)} %param.43) | copy-start | bytes 6291460
  55.1 3.2 %copy-start.4 = (bf16[128,2048]{1,0:T(8,128)(2,1)S(1)}, bf16[128,2048]{1,0:T(8,128)(2,1)}, u32[]{:S(2)}) copy-start(bf16[128,2048]{1,0:T(8,128)(2,1)} %param.36) | copy-start | bytes 1572868
  55.1 3.2 %copy-start.5 = (f32[2048]{0:T(1024)S(1)}, f32[2048]{0:T(1024)}, u32[]{:S(2)}) copy-start(f32[2048]{0:T(1024)} %param.37) | copy-start | bytes 24580
  58.2 0.7 copy-start.6
  58.2 1.7 copy-start.8
  58.2 3.7 %copy-start.9 = (f32[128,4]{0,1:T(4,128)S(1)}, f32[128,4]{0,1:T(4,128)}, u32[]{:S(2)}) copy-start(f32[128,4]{0,1:T(4,128)} %param.47) | copy-start | bytes 6148
  140.0 4.8 %copy-start.10 = (bf16[2,16,48,2048]{3,2,1,0:T(8,128)(2,1)S(1)}, bf16[2,16,48,2048]{3,2,1,0:T(8,128)(2,1)}, u32[]{:S(2)}) copy-start(bf16[2,16,48,2048]{3,2,1,0:T(8,128)(2,1)} %get-tuple-element.7) | copy-start | bytes 18874372
  140.0 5.2 %copy-start.11 = (bf16[2,2048,256]{2,1,0:T(8,128)(2,1)S(1)}, bf16[2,2048,256]{2,1,0:T(8,128)(2,1)}, u32[]{:S(2)}) copy-start(bf16[2,2048,256]{2,1,0:T(8,128)(2,1)} %param.44) | copy-start | bytes 6291460
  145.2 2.2 copy-start.3
  153.2 77.6 %copy-start.1 = (bf16[128,2048]{1,0:T(8,128)(2,1)S(1)}, bf16[128,2048]{1,0:T(8,128)(2,1)}, u32[]{:S(2)}) copy-start(bf16[128,2048]{1,0:T(8,128)(2,1)} %fusion.19.normed_ref) | copy-start | bytes 1572868
  153.2 77.6 %copy-start.2 = (bf16[2048,512]{1,0:T(8,128)(2,1)S(1)}, bf16[2048,512]{1,0:T(8,128)(2,1)}, u32[]{:S(2)}) copy-start(bf16[2048,512]{1,0:T(8,128)(2,1)} %param.40) | copy-start | bytes 6291460
  231.3 4.4 %copy-start.7 = (f32[2048]{0:T(1024)S(1)}, f32[2048]{0:T(1024)}, u32[]{:S(2)}) copy-start(f32[2048]{0:T(1024)} %param.39) | copy-start | bytes 24580
